TPU v7x, 128 devices: a whole 4x4x4 slice. The times are simulated.
128 devices in a mesh: ep: 32 (over z, y, core), tp: 4 (over x).
Axes of the slice: x: 4, y: 4, z: 4, core: 2. Of those that a mesh axis runs over, the one named last changes fastest.
Arguments:
- query_rows: bfloat16 [8192, 2048], P('ep', 'tp'), may hold values from -6 to 6
- key_rows: bfloat16 [8192, 512], P('ep', 'tp'), may hold values from -18 to 18
- value_rows: bfloat16 [8192, 512], P('ep', 'tp'), may hold values from -12 to 12
- key_bias: bfloat16 [8192, 8], P('ep', 'tp'), may hold values from -2 to 13
- head_offset: float32 [32], P('tp'), may hold values from -16 to -3
- out_weight: bfloat16 [2048, 2048], P('tp'), may hold values from -0.125 to 0.125
- expert_input: bfloat16 [16384, 2048], P(('ep', 'tp')), may hold values from -40 to 40
- expert_gain: float32 [2048], replicated, may hold values from 0.1 to 1.9
- routes: int32 [16384, 2], P(('ep', 'tp')), may hold values from 0 to 31, all different within a row; in each aligned block of 128 rows (0 to 127, 128 to 255, ...) at most 12 rows name the same one
- route_weight: float32 [16384, 2], P(('ep', 'tp')), may hold values from 0.5 to 2
- gate_weight: bfloat16 [32, 2048, 3584], P('ep', None, 'tp'), may hold values from -0.125 to 0.125
- up_weight: bfloat16 [32, 2048, 3584], P('ep', None, 'tp'), may hold values from -0.125 to 0.125
- down_weight: bfloat16 [32, 3584, 2048], P('ep', 'tp'), may hold values from -0.09375 to 0.09375
Outputs:
- mixed_a: bfloat16 [8192, 2048], P(('ep', 'tp'))
- mixed_b: bfloat16 [16384, 2048], P(('ep', 'tp'))
Inputs may be any that keep to these rules, and one draw needn't show every extreme that they name: `routes`: each row names 2 different experts; in the rows of one device (aligned blocks of 128 rows) no expert is named more than 12 times, and in every draw some device names some expert exactly 12 times.
All inputs are finite; a program needn't handle non-finite values.
Results may differ from a plain program's by a relative error of at most 0.012.
Values may be sent and summed in bfloat16 or wider, within the bound.
A program may use at most 128 MiB of HBM per device.

v0:
```python
import math

import jax
import jax.numpy as jnp
from jax import lax
from jax.sharding import PartitionSpec as P

HD = 64


EPSILON = 1e-06


def side_by_side(arrays, axis, dim, along):
    both = jnp.concatenate(arrays, axis=along)
    out, at, done = (lax.all_gather(both, axis, axis=dim, tiled=True), 0, [])
    for a in arrays:
        done.append(lax.slice_in_dim(out, at, at + a.shape[along], axis=along))
        at += a.shape[along]
    return tuple(done)


def split_up(array, dim, count):
    lengths = array.shape
    tiles = array.reshape(*lengths[:dim], count, lengths[dim] // count, *lengths[dim + 1 :])
    return jnp.moveaxis(tiles, dim, 0)


def sent_and_summed(array, axis, dim):
    tiles = split_up(array, dim, lax.axis_size(axis))
    arrived = lax.all_to_all(tiles, axis, split_axis=0, concat_axis=0, tiled=True)
    return arrived.astype(jnp.float32).sum(axis=0)


def rms_normed(rows, gain):
    values = rows.astype(jnp.float32)
    scaled = values * lax.rsqrt(jnp.mean(values * values, axis=-1, keepdims=True) + EPSILON)
    return (scaled * gain).astype(jnp.bfloat16)


def stick_update(running, queries4, key_tile_rows, value_block, bias_block, keep_mask, offsets):
    summed, survive = running
    kv_local = offsets.shape[0]
    key_heads = key_tile_rows.reshape(key_tile_rows.shape[0], kv_local, -1)
    value_heads = value_block.reshape(value_block.shape[0], kv_local, -1)
    head_dim = key_heads.shape[2]
    scores = jnp.einsum(
        "qgjd,kgd->gjqk", queries4, key_heads, preferred_element_type=jnp.float32
    ) * (1.0 / math.sqrt(head_dim))
    scores = (
        scores
        + offsets[:, :, None, None]
        + jnp.transpose(bias_block.astype(jnp.float32))[:, None, None, :]
    )
    log_stay = jnp.where(keep_mask, jax.nn.log_sigmoid(-scores), 0.0)
    after_sum = lax.cumsum(log_stay, axis=3, reverse=True) - log_stay + survive[..., None]
    weights = jnp.where(keep_mask, jnp.exp(jax.nn.log_sigmoid(scores) + after_sum), 0.0).astype(
        jnp.bfloat16
    )
    summed = summed + jnp.einsum(
        "gjqk,kgd->qgjd", weights, value_heads, preferred_element_type=jnp.float32
    )
    return (summed, survive + jnp.sum(log_stay, axis=3))


def body(
    query_rows,
    key_rows,
    value_rows,
    key_bias,
    head_offset,
    out_weight,
    expert_input,
    expert_gain,
    routes,
    route_weight,
    gate_weight,
    up_weight,
    down_weight,
):
    tok_rows = query_rows.shape[0]
    kv_local = key_rows.shape[1] // HD
    group_size = query_rows.shape[1] // key_rows.shape[1]
    offsets = head_offset.reshape(kv_local, group_size)
    all_keys, all_values, all_bias = side_by_side((key_rows, value_rows, key_bias), "ep", 0, 1)
    key_span = min(512, all_keys.shape[0])
    position = lax.axis_index("ep") * tok_rows
    block_rows = query_rows.shape[0]
    queries4 = query_rows.reshape(block_rows, kv_local, group_size, HD)
    local_index = jnp.arange(block_rows)
    running = (
        jnp.zeros((block_rows, kv_local, group_size, HD), jnp.float32),
        jnp.zeros((kv_local, group_size, block_rows), jnp.float32),
    )
    own_keys = lax.dynamic_slice_in_dim(all_keys, position, block_rows, 0)
    own_values = lax.dynamic_slice_in_dim(all_values, position, block_rows, 0)
    own_bias = lax.dynamic_slice_in_dim(all_bias, position, block_rows, 0)
    running = stick_update(
        running,
        queries4,
        own_keys,
        own_values,
        own_bias,
        local_index[None, :] < local_index[:, None],
        offsets,
    )
    block_count = (position + key_span - 1) // key_span

    def remote_block(block_turn, state_pair):
        upper_row = position - block_turn * key_span
        first_row = jnp.maximum(upper_row - key_span, 0)
        key_tile_rows = lax.dynamic_slice_in_dim(all_keys, first_row, key_span, 0)
        value_block = lax.dynamic_slice_in_dim(all_values, first_row, key_span, 0)
        bias_block = lax.dynamic_slice_in_dim(all_bias, first_row, key_span, 0)
        keep_mask = jnp.broadcast_to(
            (first_row + jnp.arange(key_span) < upper_row)[None, :], (block_rows, key_span)
        )
        return stick_update(
            state_pair, queries4, key_tile_rows, value_block, bias_block, keep_mask, offsets
        )

    running = lax.fori_loop(0, block_count, remote_block, running)
    heads_out = running[0].reshape(block_rows, -1).astype(jnp.bfloat16)
    mixed_a = sent_and_summed(
        jnp.dot(heads_out, out_weight, preferred_element_type=jnp.float32).astype(jnp.bfloat16),
        "tp",
        0,
    ).astype(jnp.bfloat16)
    normed = rms_normed(expert_input, expert_gain)
    tok_count = normed.shape[0]
    top_count = routes.shape[1]
    model_width = normed.shape[1]
    expert_count = lax.axis_size("ep")
    capacity = max(2, 3 * tok_count * top_count // (2 * expert_count))
    flat_route = routes.reshape(-1)
    one_hot = (flat_route[:, None] == jnp.arange(expert_count)[None, :]).astype(jnp.int32)
    before = jnp.cumsum(one_hot, axis=0) - one_hot
    slot_index = (flat_route * capacity + jnp.sum(before * one_hot, axis=1)).reshape(
        tok_count, top_count
    )
    slot_ids = jnp.arange(expert_count * capacity)
    dispatch = jnp.sum(
        (slot_index[None, :, :] == slot_ids[:, None, None]).astype(jnp.int32), axis=2
    ).astype(jnp.bfloat16)
    outgoing = (
        jnp.dot(dispatch, normed, preferred_element_type=jnp.float32)
        .astype(jnp.bfloat16)
        .reshape(expert_count, capacity, model_width)
    )
    source_rows = expert_count * capacity
    arrived = lax.all_to_all(outgoing, "ep", split_axis=0, concat_axis=0, tiled=True)
    row_piece = lax.all_gather(arrived.reshape(source_rows, model_width), "tp", axis=0, tiled=True)
    gate_act = jnp.dot(row_piece, gate_weight[0], preferred_element_type=jnp.float32)
    up_act = jnp.dot(row_piece, up_weight[0], preferred_element_type=jnp.float32)
    hidden_all = (jax.nn.silu(gate_act) * up_act).astype(jnp.bfloat16)
    expert_result = sent_and_summed(
        jnp.dot(hidden_all, down_weight[0], preferred_element_type=jnp.float32).astype(
            jnp.bfloat16
        ),
        "tp",
        0,
    ).astype(jnp.bfloat16)
    returned = lax.all_to_all(
        expert_result.reshape(expert_count, capacity, model_width),
        "ep",
        split_axis=0,
        concat_axis=0,
        tiled=True,
    )
    picked_rows = returned.reshape(-1, model_width)[slot_index.reshape(-1)].reshape(
        tok_count, top_count, model_width
    )
    mixed_b = jnp.sum(picked_rows.astype(jnp.float32) * route_weight[:, :, None], axis=1).astype(
        jnp.bfloat16
    )
    return (mixed_a, mixed_b)


def solution(mesh):
    return jax.shard_map(
        body,
        mesh=mesh,
        in_specs=(
            P("ep", "tp"),
            P("ep", "tp"),
            P("ep", "tp"),
            P("ep", "tp"),
            P("tp"),
            P("tp", None),
            P(("ep", "tp"), None),
            P(),
            P(("ep", "tp"), None),
            P(("ep", "tp"), None),
            P("ep", None, "tp"),
            P("ep", None, "tp"),
            P("ep", "tp", None),
        ),
        out_specs=(P(("ep", "tp"), None), P(("ep", "tp"), None)),
        check_vma=False,
    )
```

profile of v0, /device:TPU:1, one launch (start us, length us, event | category | flops | bytes accessed | tf_op | source)
XLA Modules:
  0.0 882.6 jit_solution(11130264866837876475)
XLA Ops:
  7.2 1.1 copy.44
  8.3 0.9 copy.43
  9.3 1.3 pad_maximum_fusion
  10.7 0.8 copy.49
  11.8 0.6 reduce-window.38
  13.0 1.2 fusion.35
  14.2 2.9 convolution_convert_fusion.1
  17.1 3.6 reshape.159
  20.7 38.4 %all_to_all.20 = bf16[32,12,2048]{2,1,0:T(8,128)(2,1)} all-to-all(bf16[32,12,2048]{2,1,0:T(8,128)(2,1)} %reshape.159), channel_id=1, replica_groups=mesh['ep'=32,'tp'=4] {'ep'}, dimensions={0} | all-to-all | bytes 3145728 | tf_op jit(solution)/shard_map/all_to_all | solution.py:151
  59.0 4.1 reshape.160
  63.5 10.3 %all-gather.3.cloned.1.call-done = bf16[8192,258]{0,1:T(8,128)(2,1)} async-done(((bf16[256,258]{0,1:T(8,128)(2,1)}), bf16[8192,258]{0,1:T(8,128)(2,1)}) %all-gather.3.cloned.1.call-update) | async-done | bytes 4227088 | tf_op jit(solution)/shard_map/all_gather | solution.py:16
  73.8 0.9 slice.46
  74.7 2.7 fusion.51
  77.4 3.1 fusion.48
  80.5 18.5 %fusion.33 = f32[2,4,256,2,128]{2,3,4,1,0:T(2,128)S(1)} fusion(f32[2,4,256,2,128]{2,4,3,1,0:T(8,128)S(1)} %bitcast.166), kind=kOutput, calls=%fused_computation.56 | output fusion | flops 66584576 | bytes 4194304 | tf_op jit(solution)/shard_map/reduce-window.2
  99.1 1.3 copy-done.5
  100.4 2.3 broadcast_add_fusion.1
  103.0 1.4 copy-done.8
  104.4 3.6 fusion.26
  108.0 0.3 convolution_bitcast_fusion.1
  108.3 31.4 %all-gather.5.cloned.1.call-done = bf16[1536,2048]{1,0:T(8,128)(2,1)} async-done(((bf16[384,2048]{1,0:T(8,128)(2,1)}), bf16[1536,2048]{1,0:T(8,128)(2,1)}) %all-gather.5.cloned.1.call-update) | async-done | bytes 6291472 | tf_op jit(solution)/shard_map/all_gather | solution.py:152
  139.7 11.3 %fusion.19 = f32[1536,896]{1,0:T(8,128)} fusion(bf16[1536,2048]{1,0:T(8,128)(2,1)} %all-gather.5.cloned.1.call-done, bf16[1,2048,896]{2,1,0:T(8,128)(2,1)} %param.25), kind=kOutput, calls=%fused_computation.36 | convolution fusion | flops 5637144576 | bytes 15466496 | tf_op jit(solution)/shard_map/dot_general | solution.py:153
  151.0 20.1 %convolution_convert_fusion = bf16[1536,2048]{1,0:T(8,128)(2,1)} fusion(bf16[1,896,2048]{2,1,0:T(8,128)(2,1)} %param.27, f32[1536,896]{1,0:T(8,128)} %fusion.19, bf16[1536,2048]{1,0:T(8,128)(2,1)} %all-gather.5.cloned.1.call-done, bf16[1,2048,896]{2,1,0:T(8,128)(2,1)} %param.26), kind=kOutput, calls=%fused_computation.30 | convolution fusion | flops 11285692416 | bytes 25427968 | tf_op jit(solution)/shard_map/dot_general | solution.py:157
  171.1 5.2 all-to-all-start.2
  176.4 46.6 %while.14 = (s32[]{:T(128)}, f32[256,2,4,64]{0,3,2,1:T(8,128)S(1)}, f32[2,4,256]{2,1,0:T(4,128)S(1)}, s32[]{:T(128)}, s32[]{:T(128)}, /*index=5*/bf16[8192,128]{...) while((s32[]{:T(128)}, f32[256,2,4,64]{0,3,2,1:T(8,128)S(1)}, ...), condition=%wide.region_7.8_spmd, body=%wide.region_3.7_spmd.sunk | while | flops 432177152 | bytes 119832520 | solution.py:122
  176.6 1.1 constant_dynamic-slice_fusion.5
  177.9 5.0 fusion.78
  182.9 19.4 %fusion.79 = f32[2,4,256,4,128]{2,3,4,1,0:T(4,128)S(1)} fusion(f32[2,4,256,4,128]{2,4,3,1,0:T(8,128)S(1)} %bitcast.161), kind=kOutput, calls=%fused_computation.19.clone.1 | output fusion | flops 133169152 | bytes 8388608 | tf_op jit(solution)/shard_map/reduce-window.10
  202.3 2.0 copy-done.1
  204.3 2.9 broadcast_add_fusion.3
  207.3 0.7 copy.70
  208.0 1.4 copy-done.3
  209.5 1.3 copy-done.4
  210.7 4.3 fusion.80
  215.1 0.5 fusion.81
  223.1 1.8 convolution_convert_fusion.2
  224.9 22.1 %all-to-all-done.2 = bf16[4,384,2048]{2,1,0:T(8,128)(2,1)} async-done(((bf16[4,384,2048]{2,1,0:T(8,128)(2,1)}), bf16[4,384,2048]{2,1,0:T(8,128)(2,1)}, u32[]{:S(2)}, u32[]{:S(2)}) %all-to-all-start.2) | async-done | bytes 6291488 | tf_op jit(solution)/shard_map/all_to_all | solution.py:31
  247.0 3.5 all-to-all-start
  250.5 5.7 reduce_sum.91
  256.2 3.6 reshape.162
  259.8 4.2 all-to-all-done
  264.0 567.3 %all-to-all-start.3 = ((bf16[32,12,2048]{2,1,0:T(8,128)(2,1)}), bf16[32,12,2048]{2,1,0:T(8,128)(2,1)}, u32[]{:S(2)}, u32[]{:S(2)}) async-start(bf16[32,12,2048]{2,1,0:T(8,128)(2,1)} %reshape.162), calls=%async_computation.3 | async-start | bytes 4194304 | tf_op jit(solution)/shard_map/all_to_all | solution.py:163
  831.5 0.9 reduce_sum.86
  832.4 27.5 %all-to-all-done.3 = bf16[32,12,2048]{2,1,0:T(8,128)(2,1)} async-done(((bf16[32,12,2048]{2,1,0:T(8,128)(2,1)}), bf16[32,12,2048]{2,1,0:T(8,128)(2,1)}, u32[]{:S(2)}, u32[]{:S(2)}) %all-to-all-start.3) | async-done | bytes 1572896 | tf_op jit(solution)/shard_map/all_to_all | solution.py:163
  860.0 3.6 reshape.163
  863.6 4.0 gather_fusion
  867.6 2.4 reshape.164
  869.9 5.6 multiply_reduce_fusion
  (56 shorter events, 2.2 us)
Async XLA Ops:
  7.2 215.9 %copy-start = (bf16[512,2048]{1,0:T(8,128)(2,1)S(1)}, bf16[512,2048]{1,0:T(8,128)(2,1)}, u32[]{:S(2)}) copy-start(bf16[512,2048]{1,0:T(8,128)(2,1)} %param.20) | copy-start | bytes 6291460
  7.2 66.6 %all-gather.3.cloned.1.call-start = ((), (), s32[]{:S(2)}) async-start(), calls=%async_computation.4 | async-start | bytes 4460544 | tf_op jit(solution)/shard_map/all_gather | solution.py:16
  10.6 129.1 %all-gather.5.cloned.1.call-start = ((), (), s32[]{:S(2)}) async-start(), calls=%async_computation.5 | async-start | bytes 7864320 | tf_op jit(solution)/shard_map/all_gather | solution.py:152
  59.0 4.2 copy-start.11
  59.0 4.2 copy-start.9
  77.4 3.1 copy-start.6
  77.4 3.1 copy-start.7
  99.1 1.3 copy-start.5
  102.8 1.6 copy-start.8
  171.1 75.8 %all-to-all-start.2 = ((bf16[4,384,2048]{2,1,0:T(8,128)(2,1)}), bf16[4,384,2048]{2,1,0:T(8,128)(2,1)}, u32[]{:S(2)}, u32[]{:S(2)}) async-start(bf16[4,384,2048]{2,1,0:T(8,128)(2,1)} %bitcast.163), calls=%async_computation.2 | async-start | bytes 12582912 | tf_op jit(solution)/shard_map/all_to_all | solution.py:31
  182.9 19.4 %copy-start.2 = (f32[2,4,256,512]{2,3,1,0:T(8,128)}, f32[2,4,256,512]{2,3,1,0:T(8,128)S(1)}, u32[]{:S(2)}) copy-start(f32[2,4,256,512]{2,3,1,0:T(8,128)S(1)} %get-tuple-element.234) | copy-start | bytes 12582916 | tf_op jit(solution)/shard_map/while
  202.3 2.0 copy-start.1
  207.3 2.2 copy-start.3
  207.3 3.5 copy-start.4
  247.0 17.0 %all-to-all-start = ((bf16[4,64,2048]{2,1,0:T(8,128)(2,1)}), bf16[4,64,2048]{2,1,0:T(8,128)(2,1)S(1)}, u32[]{:S(2)}, u32[]{:S(2)}) async-start(bf16[4,64,2048]{2,1,0:T(8,128)(2,1)} %bitcast.164), calls=%async_computation | async-start | bytes 2097152 | tf_op jit(solution)/shard_map/all_to_all | solution.py:31
  256.2 575.2 %copy-start.10 = (f32[128,2]{0,1:T(2,128)S(1)}, f32[128,2]{0,1:T(2,128)}, u32[]{:S(2)}) copy-start(f32[128,2]{0,1:T(2,128)} %param.24) | copy-start | bytes 3076
  264.0 596.0 %all-to-all-start.3 = ((bf16[32,12,2048]{2,1,0:T(8,128)(2,1)}), bf16[32,12,2048]{2,1,0:T(8,128)(2,1)}, u32[]{:S(2)}, u32[]{:S(2)}) async-start(bf16[32,12,2048]{2,1,0:T(8,128)(2,1)} %reshape.162), calls=%async_computation.3 | async-start | bytes 4194304 | tf_op jit(solution)/shard_map/all_to_all | solution.py:163
Sparse Core Ops, SparseCore 0:
  10.7 62.9 all-gather.2
  75.5 64.1 all-gather.4
where the time goes:
time: 887 us; the launch traced here: 883 us
  starting transfers between devices  576 us (65%)
  waiting for transfers between devices  95.6 us (11%)
  other arithmetic  67 us (8%)
  matrix products  44.9 us (5%)
  local copies, waits for them, and re-layouts  38.4 us (4%)
  blocking collectives  38.4 us (4%)
  between operations  14.5 us (2%)
    all_to_all x1, starting transfers between devices, body(): lax.all_to_all(expert_result.reshape(expert_count, capacity, model_width)...  567 us
    another operation x6, other arithmetic  38.7 us
    all_to_all x1, blocking collectives, body(): lax.all_to_all(outgoing, 'ep', split_axis=0, concat_axis=0, tiled=True)  38.4 us
    all_gather x1, waiting for transfers between devices, body(): lax.all_gather(arrived.reshape(source_rows, model_width), 'tp', axis=0, t...  31.4 us
    all_to_all x1, waiting for transfers between devices, body(): lax.all_to_all(expert_result.reshape(expert_count, capacity, model_width)...  27.5 us
    all_to_all x2, waiting for transfers between devices, sent_and_summed(): lax.all_to_all(tiles, axis, split_axis=0, concat_axis=0, tiled=True)  26.3 us
    dot_general x1, matrix products, body(): jnp.dot(hidden_all, down_weight[0], preferred_element_type=jnp.float32)  20.1 us
  transfers between devices with their start and end apart: 5, of which 5 were waited for; matrix products, arithmetic and copies ran while one was open for 10% of the time, Pallas kernels for 0%

commit v1 on v0

v1 whole, which is shorter than its diff:
```python
import functools
import math

import jax
import jax.numpy as jnp
from jax import lax
from jax.experimental import pallas as pl
from jax.experimental.pallas import tpu as pltpu
from jax.sharding import PartitionSpec as P

HD = 64
BLK = 256
EPSILON = 1e-06
TO_LOG2 = math.log2(math.e) / math.sqrt(HD)


def rms_normed(rows, gain):
    values = rows.astype(jnp.float32)
    scaled = values * lax.rsqrt(jnp.mean(values * values, axis=-1, keepdims=True) + EPSILON)
    return (scaled * gain).astype(jnp.bfloat16)


def stick_kernel(count_ref, q_ref, kv_ref, o_ref, acc, surv, tri, *, tile):
    count = count_ref[0]
    rows = q_ref.shape[1]
    at_row = lax.broadcasted_iota(jnp.int32, (BLK, BLK), 0)
    at_col = lax.broadcasted_iota(jnp.int32, (BLK, BLK), 1)
    tri[...] = jnp.where(at_row > at_col, -1.0, 0.0).astype(jnp.bfloat16)
    acc[...] = jnp.zeros_like(acc)
    surv[...] = jnp.zeros_like(surv)

    def block(index, diagonal):
        at = pl.multiple_of(index * BLK, BLK)
        keys = kv_ref[pl.ds(at, BLK), 0:256]
        for g in range(2):
            vals = kv_ref[pl.ds(at, BLK), 256 + HD * g : 256 + HD * (g + 1)]
            for m in range(rows // tile):
                part = slice(m * tile, (m + 1) * tile)
                z = (
                    lax.dot_general(
                        q_ref[g, part, :],
                        keys,
                        (((1,), (1,)), ((), ())),
                        preferred_element_type=jnp.float32,
                    )
                    * TO_LOG2
                )
                if diagonal:
                    query = lax.broadcasted_iota(jnp.int32, (tile, BLK), 0) % BLK
                    key = lax.broadcasted_iota(jnp.int32, (tile, BLK), 1)
                    z = jnp.where(key < query, z, -1e30)
                leave = jnp.maximum(z, jnp.log2(1.0 + jnp.exp2(jnp.minimum(z, 100.0))))
                after = (
                    jnp.dot(
                        leave.astype(jnp.bfloat16), tri[...], preferred_element_type=jnp.float32
                    )
                    - leave
                )
                s = surv[g, part, :]
                w = jnp.exp2(z + after + jnp.concatenate([s, s], axis=1)).astype(jnp.bfloat16)
                acc[g, part, :] += jnp.dot(w, vals, preferred_element_type=jnp.float32)
                surv[g, part, :] = s + jnp.broadcast_to(after[:, 0:1], s.shape)

    block(count - 1, True)

    def step(i, _):
        block(count - 2 - i, False)
        return 0

    lax.fori_loop(0, count - 1, step, 0)
    o_ref[...] = acc[...].astype(jnp.bfloat16)


def attention(count, q_aug, kv, tile=512):
    rows = q_aug.shape[1]
    return pl.pallas_call(
        functools.partial(stick_kernel, tile=tile),
        out_shape=jax.ShapeDtypeStruct((2, rows, HD), jnp.bfloat16),
        in_specs=[
            pl.BlockSpec(memory_space=pltpu.SMEM),
            pl.BlockSpec(memory_space=pltpu.VMEM),
            pl.BlockSpec(memory_space=pltpu.VMEM),
        ],
        out_specs=pl.BlockSpec(memory_space=pltpu.VMEM),
        scratch_shapes=[
            pltpu.VMEM((2, rows, HD), jnp.float32),
            pltpu.VMEM((2, rows, 128), jnp.float32),
            pltpu.VMEM((BLK, BLK), jnp.bfloat16),
        ],
        compiler_params=pltpu.CompilerParams(vmem_limit_bytes=40 * 1024 * 1024),
        cost_estimate=pl.CostEstimate(
            flops=40_000_000_000, bytes_accessed=8_000_000, transcendentals=100_000_000
        ),
        name="stick",
    )(count, q_aug, kv)


def augment_q(q, offs):
    R = q.shape[0]
    q4 = q.reshape(R, 2, 4, HD).transpose(1, 2, 0, 3).reshape(2, 4 * R, HD)
    rest = offs * 8.0
    terms = []
    for _ in range(3):
        term = rest.astype(jnp.bfloat16)
        terms.append(term)
        rest = rest - term.astype(jnp.float32)
    terms = jnp.stack(terms, 1).reshape(2, 4, 3)
    terms = jnp.broadcast_to(terms[:, :, None, :], (2, 4, R, 3)).reshape(2, 4 * R, 3)
    zeros = jnp.zeros((4 * R, HD), jnp.bfloat16)
    one = jnp.ones((4 * R, 1), jnp.bfloat16)
    none = jnp.zeros((4 * R, 1), jnp.bfloat16)
    tail = jnp.zeros((4 * R, 123), jnp.bfloat16)
    return jnp.stack(
        [
            jnp.concatenate([q4[0], zeros, one, none, terms[0], tail], 1),
            jnp.concatenate([zeros, q4[1], none, one, terms[1], tail], 1),
        ]
    )


def augment_kv(k, v, b):
    R = k.shape[0]
    return jnp.concatenate(
        [k, b * 8, jnp.ones((R, 3), jnp.bfloat16), jnp.zeros((R, 123), jnp.bfloat16), v], 1
    )


def body(
    query_rows,
    key_rows,
    value_rows,
    key_bias,
    head_offset,
    out_weight,
    expert_input,
    expert_gain,
    routes,
    route_weight,
    gate_weight,
    up_weight,
    down_weight,
):
    block_rows = query_rows.shape[0]
    all_kv = lax.all_gather(
        augment_kv(key_rows, value_rows, key_bias), "ep", axis=0, tiled=True
    )
    count = (lax.axis_index("ep") + 1).astype(jnp.int32).reshape(1)
    stacked = attention(count, augment_q(query_rows, head_offset), all_kv)
    heads_out = (
        stacked.reshape(8, block_rows, HD).transpose(1, 0, 2).reshape(block_rows, 8 * HD)
    )
    mixed_a = lax.psum_scatter(
        jnp.dot(heads_out, out_weight, preferred_element_type=jnp.float32).astype(jnp.bfloat16),
        "tp",
        scatter_dimension=0,
        tiled=True,
    )
    normed = rms_normed(expert_input, expert_gain)
    tok_count = normed.shape[0]
    top_count = routes.shape[1]
    model_width = normed.shape[1]
    expert_count = lax.axis_size("ep")
    capacity = max(2, 3 * tok_count * top_count // (2 * expert_count))
    flat_route = routes.reshape(-1)
    one_hot = (flat_route[:, None] == jnp.arange(expert_count)[None, :]).astype(jnp.int32)
    before = jnp.cumsum(one_hot, axis=0) - one_hot
    slot_index = (flat_route * capacity + jnp.sum(before * one_hot, axis=1)).reshape(
        tok_count, top_count
    )
    slot_ids = jnp.arange(expert_count * capacity)
    dispatch = jnp.sum(
        (slot_index[None, :, :] == slot_ids[:, None, None]).astype(jnp.int32), axis=2
    ).astype(jnp.bfloat16)
    outgoing = (
        jnp.dot(dispatch, normed, preferred_element_type=jnp.float32)
        .astype(jnp.bfloat16)
        .reshape(expert_count, capacity, model_width)
    )
    source_rows = expert_count * capacity
    arrived = lax.all_to_all(outgoing, "ep", split_axis=0, concat_axis=0, tiled=True)
    row_piece = lax.all_gather(arrived.reshape(source_rows, model_width), "tp", axis=0, tiled=True)
    gate_act = jnp.dot(row_piece, gate_weight[0], preferred_element_type=jnp.float32)
    up_act = jnp.dot(row_piece, up_weight[0], preferred_element_type=jnp.float32)
    hidden_all = (jax.nn.silu(gate_act) * up_act).astype(jnp.bfloat16)
    expert_result = lax.psum_scatter(
        jnp.dot(hidden_all, down_weight[0], preferred_element_type=jnp.float32).astype(
            jnp.bfloat16
        ),
        "tp",
        scatter_dimension=0,
        tiled=True,
    )
    returned = lax.all_to_all(
        expert_result.reshape(expert_count, capacity, model_width),
        "ep",
        split_axis=0,
        concat_axis=0,
        tiled=True,
    )
    picked_rows = returned.reshape(-1, model_width)[slot_index.reshape(-1)].reshape(
        tok_count, top_count, model_width
    )
    mixed_b = jnp.sum(picked_rows.astype(jnp.float32) * route_weight[:, :, None], axis=1).astype(
        jnp.bfloat16
    )
    return (mixed_a, mixed_b)


def solution(mesh):
    return jax.shard_map(
        body,
        mesh=mesh,
        in_specs=(
            P("ep", "tp"),
            P("ep", "tp"),
            P("ep", "tp"),
            P("ep", "tp"),
            P("tp"),
            P("tp", None),
            P(("ep", "tp"), None),
            P(),
            P(("ep", "tp"), None),
            P(("ep", "tp"), None),
            P("ep", None, "tp"),
            P("ep", None, "tp"),
            P("ep", "tp", None),
        ),
        out_specs=(P(("ep", "tp"), None), P(("ep", "tp"), None)),
        check_vma=False,
    )
```

time: 887 us -> 303 us (0.34)
  starting transfers between devices: 576 us -> 7.98 us
  waiting for transfers between devices: 95.6 us -> 157 us
  other arithmetic: 67 us -> 9 us
    all_to_all x1, starting transfers between devices: 567 us -> 7.82 us  [body(): lax.all_to_all(expert_result.reshape(expert_count, capacity, model_width)...]
    reduce_scatter x0 -> x2, waiting for transfers between devices: none -> 54.8 us  [the longest x1 54.8 us: body(): lax.psum_scatter(jnp.dot(hidden_all, down_weight[0], preferred_element_ty...]
    another operation x8 -> x3, other arithmetic: 43.9 us -> 1.97 us  [the longest x1 1.34 us: augment_q(): jnp.stack([jnp.concatenate([q4[0], zeros, one, none, terms[0], tail], 1),...]
    all_gather x1, waiting for transfers between devices: 31.4 us -> 61.9 us  [body(): lax.all_gather(arrived.reshape(source_rows, model_width), 'tp', axis=0, t...]
    all_to_all x2 -> x0, waiting for transfers between devices: 26.3 us -> none  [sent_and_summed(): lax.all_to_all(tiles, axis, split_axis=0, concat_axis=0, tiled=True)]
  transfers between devices with their start and end apart: 5 -> 5, of which waited for: 5 -> 4; matrix products, arithmetic and copies ran while one was open for 10% -> 21% of each run, Pallas kernels for 0% -> 1%
where the time goes in v1:
time: 303 us; the launch traced here: 302 us
  waiting for transfers between devices  157 us (52%)
  blocking collectives  38 us (13%)
  matrix products  36.2 us (12%)
  local copies, waits for them, and re-layouts  35.9 us (12%)
  between operations  14 us (5%)
  other arithmetic  9 us (3%)
  starting transfers between devices  7.98 us (3%)
  Pallas kernels  3.19 us (1%)
    all_gather x1, waiting for transfers between devices, body(): lax.all_gather(arrived.reshape(source_rows, model_width), 'tp', axis=0, t...  61.9 us
    reduce_scatter x1, waiting for transfers between devices, body(): lax.psum_scatter(jnp.dot(hidden_all, down_weight[0], preferred_element_ty...  54.8 us
    all_to_all x1, blocking collectives, body(): lax.all_to_all(outgoing, 'ep', split_axis=0, concat_axis=0, tiled=True)  38 us
    all_to_all x1, waiting for transfers between devices, body(): lax.all_to_all(expert_result.reshape(expert_count, capacity, model_width)...  28.4 us
    dot_general x1, matrix products, body(): jnp.dot(hidden_all, down_weight[0], preferred_element_type=jnp.float32)  20.3 us
    all_gather x1, waiting for transfers between devices, body(): lax.all_gather(augment_kv(key_rows, value_rows, key_bias), 'ep', axis=0,...  12.1 us
    dot_general x1, matrix products, body(): jnp.dot(row_piece, gate_weight[0], preferred_element_type=jnp.float32)  11.4 us
    all_to_all x1, starting transfers between devices, body(): lax.all_to_all(expert_result.reshape(expert_count, capacity, model_width)...  7.82 us
  transfers between devices with their start and end apart: 5, of which 4 were waited for; matrix products, arithmetic and copies ran while one was open for 21% of the time, Pallas kernels for 1%

profile of v1, /device:TPU:1, one launch (start us, length us, event | category | flops | bytes accessed | tf_op | source)
XLA Modules:
  0.0 301.6 jit_solution(6017037985870654238)
XLA Ops:
  7.2 0.9 copy.56
  8.2 0.1 eq.42
  8.3 0.1 eq.38
  8.4 0.6 reduce-window.6
  9.0 0.2 slice_reduce_fusion
  9.3 0.1 fusion.16
  9.4 0.1 reduce_sum.41
  9.5 0.1 copy.60
  9.6 0.1 convert_reduce_fusion
  9.7 1.2 fusion.7
  10.9 2.9 convolution_convert_fusion.1
  13.8 3.6 %reshape.122 = bf16[32,12,2048]{2,1,0:T(8,128)(2,1)} reshape(bf16[384,2048]{1,0:T(8,128)(2,1)} %convolution_convert_fusion.1) | data formatting | bytes 3145728 | tf_op jit(solution)/shard_map/reshape | solution.py:177
  17.4 38.0 %all_to_all.10 = bf16[32,12,2048]{2,1,0:T(8,128)(2,1)} all-to-all(bf16[32,12,2048]{2,1,0:T(8,128)(2,1)} %reshape.122), channel_id=1, replica_groups=mesh['ep'=32,'tp'=4] {'ep'}, dimensions={0} | all-to-all | bytes 3145728 | tf_op jit(solution)/shard_map/all_to_all | solution.py:180
  55.4 3.7 %reshape.123 = bf16[384,2048]{1,0:T(8,128)(2,1)} reshape(bf16[32,12,2048]{2,1,0:T(8,128)(2,1)} %all_to_all.10) | data formatting | bytes 3145728 | tf_op jit(solution)/shard_map/reshape | solution.py:181
  59.1 0.1 copy.54
  59.3 0.8 concatenate.12
  60.2 61.9 %all-gather.5.cloned.1.call-done = bf16[1536,2048]{1,0:T(8,128)(2,1)} async-done(((bf16[384,2048]{1,0:T(8,128)(2,1)}), bf16[1536,2048]{1,0:T(8,128)(2,1)}) %all-gather.5.cloned.1.call-update) | async-done | bytes 6291472 | tf_op jit(solution)/shard_map/all_gather | solution.py:181
  122.1 11.4 %fusion.4 = f32[1536,896]{1,0:T(8,128)} fusion(bf16[1536,2048]{1,0:T(8,128)(2,1)} %all-gather.5.cloned.1.call-done, bf16[1,2048,896]{2,1,0:T(8,128)(2,1)} %param.23), kind=kOutput, calls=%fused_computation.5 | convolution fusion | flops 5637144576 | bytes 15466496 | tf_op jit(solution)/shard_map/dot_general | solution.py:182
  133.5 20.3 %convolution_convert_fusion = bf16[1536,2048]{1,0:T(8,128)(2,1)} fusion(bf16[1,896,2048]{2,1,0:T(8,128)(2,1)} %param.25, f32[1536,896]{1,0:T(8,128)} %fusion.4, bf16[1536,2048]{1,0:T(8,128)(2,1)} %all-gather.5.cloned.1.call-done, bf16[1,2048,896]{2,1,0:T(8,128)(2,1)} %param.24), kind=kOutput, calls=%fused_computation.1 | convolution fusion | flops 11285692416 | bytes 25427968 | tf_op jit(solution)/shard_map/dot_general | solution.py:186
  153.8 0.6 copy-done.8
  154.4 0.1 stack.21
  154.5 0.1 stack.22
  154.6 0.1 stack.23
  154.7 0.1 copy.51
  154.8 0.1 copy.49
  155.0 0.2 copy.50
  155.1 0.1 copy.53
  155.2 0.8 copy.52
  156.1 0.7 broadcast_in_dim.38
  157.0 2.2 concatenate.10
  159.2 2.1 concatenate.11
  161.4 1.3 pad_maximum_fusion.q_ref
  162.7 12.1 %all-gather.3.cloned.1.call-done.kv_ref = bf16[8192,384]{1,0:T(8,128)(2,1)} async-done(((bf16[256,384]{1,0:T(8,128)(2,1)}), bf16[8192,384]{1,0:T(8,128)(2,1)}) %all-gather.3.cloned.1.call-update) | async-done | bytes 6291472 | tf_op jit(solution)/shard_map/all_gather | solution.py:144
  174.8 2.8 copy-done.2
  177.6 3.2 %stick.1 = bf16[2,1024,64]{2,1,0:T(8,128)(2,1)S(1)} custom-call(s32[1]{0:T(128)} %bitcast.count_ref, bf16[2,1024,256]{2,1,0:T(8,128)(2,1)S(1)} %pad_maximum_fusion.q_ref, bf16[8192,384]{1,0:T(8,128)(2,1)S(1)} %copy-done.2), custom_call_target="tpu_custom_call" | custom-call | flops 40000000000 | bytes 8000000 | tf_op jit(solution)/shard_map/stick/pallas_call | solution.py:76
  180.8 0.8 copy-done.1
  181.6 1.2 copy.55
  182.8 1.7 convolution_convert_fusion.2
  184.6 54.8 %reduce-scatter.5.cloned.1.call-done = bf16[384,2048]{1,0:T(8,128)(2,1)} async-done(((bf16[1536,2048]{1,0:T(8,128)(2,1)}), bf16[384,2048]{1,0:T(8,128)(2,1)}) %reduce-scatter.5.cloned.1.call-update) | async-done | bytes 1572880 | tf_op jit(solution)/shard_map/reduce_scatter | solution.py:185
  239.4 3.6 %reshape.124 = bf16[32,12,2048]{2,1,0:T(8,128)(2,1)} reshape(bf16[384,2048]{1,0:T(8,128)(2,1)} %reduce-scatter.5.cloned.1.call-done) | data formatting | bytes 3145728 | tf_op jit(solution)/shard_map/reshape | solution.py:194
  243.0 7.8 %all-to-all-start.1 = ((bf16[32,12,2048]{2,1,0:T(8,128)(2,1)}), bf16[32,12,2048]{2,1,0:T(8,128)(2,1)}, u32[]{:S(2)}, u32[]{:S(2)}) async-start(bf16[32,12,2048]{2,1,0:T(8,128)(2,1)} %reshape.124), calls=%async_computation.3 | async-start | bytes 4194304 | tf_op jit(solution)/shard_map/all_to_all | solution.py:193
  250.8 0.1 mul.77
  250.9 0.1 copy.61
  251.1 28.4 %all-to-all-done.1 = bf16[32,12,2048]{2,1,0:T(8,128)(2,1)} async-done(((bf16[32,12,2048]{2,1,0:T(8,128)(2,1)}), bf16[32,12,2048]{2,1,0:T(8,128)(2,1)}, u32[]{:S(2)}, u32[]{:S(2)}) %all-to-all-start.1) | async-done | bytes 1572896 | tf_op jit(solution)/shard_map/all_to_all | solution.py:193
  279.5 3.6 %reshape.125 = bf16[384,2048]{1,0:T(8,128)(2,1)} reshape(bf16[32,12,2048]{2,1,0:T(8,128)(2,1)} %all-to-all-done.1) | data formatting | bytes 3145728 | tf_op jit(solution)/shard_map/reshape | solution.py:200
  283.1 4.0 %gather_fusion = bf16[256,2048]{1,0:T(8,128)(2,1)S(1)} fusion(bf16[384,2048]{1,0:T(8,128)(2,1)} %reshape.125, s32[1024]{0:T(1024)S(1)} %pad_clamp_fusion), kind=kCustom, calls=%fused_computation | custom fusion | bytes 2098176 | tf_op jit(solution)/shard_map/gather | solution.py:200
  287.1 2.4 reshape.126
  289.5 5.6 %multiply_reduce_fusion = bf16[128,2048]{1,0:T(8,128)(2,1)} fusion(f32[128,2,2048]{2,1,0:T(2,128)} %reshape.126, f32[128,2]{1,0:T(8,128)S(1)} %copy.61), kind=kLoop, calls=%fused_computation.10 | loop fusion | flops 786432 | bytes 2622464 | tf_op jit(solution)/shard_map/reduce_sum | solution.py:203
  (45 shorter events, 0.6 us)
Async XLA Ops:
  7.2 175.6 %copy-start = (bf16[512,2048]{1,0:T(8,128)(2,1)S(1)}, bf16[512,2048]{1,0:T(8,128)(2,1)}, u32[]{:S(2)}) copy-start(bf16[512,2048]{1,0:T(8,128)(2,1)} %param.18) | copy-start | bytes 6291460
  7.2 114.9 %all-gather.5.cloned.1.call-start = ((), (), s32[]{:S(2)}) async-start(), calls=%async_computation.6 | async-start | bytes 7864320 | tf_op jit(solution)/shard_map/all_gather | solution.py:181
  55.4 3.7 %copy-start.7 = (bf16[256,2]{0,1:T(2,128)(2,1)S(1)}, bf16[256,2]{0,1:T(2,128)(2,1)}, u32[]{:S(2)}) copy-start(bf16[256,2]{0,1:T(2,128)(2,1)} %param.16) | copy-start | bytes 3076
  55.4 3.9 %copy-start.4 = (bf16[256,128]{1,0:T(8,128)(2,1)S(1)}, bf16[256,128]{1,0:T(8,128)(2,1)}, u32[]{:S(2)}) copy-start(bf16[256,128]{1,0:T(8,128)(2,1)} %param.14) | copy-start | bytes 196612
  55.4 3.9 %copy-start.5 = (bf16[256,128]{1,0:T(8,128)(2,1)S(1)}, bf16[256,128]{1,0:T(8,128)(2,1)}, u32[]{:S(2)}) copy-start(bf16[256,128]{1,0:T(8,128)(2,1)} %param.15) | copy-start | bytes 196612
  59.0 115.8 %all-gather.3.cloned.1.call-start = ((), (), s32[]{:S(2)}) async-start(), calls=%async_computation.4 | async-start | bytes 6488064 | tf_op jit(solution)/shard_map/all_gather | solution.py:144
  60.1 179.2 %reduce-scatter.5.cloned.1.call-start = ((), (), s32[]{:S(2)}) async-start(), calls=%async_computation.7 | async-start | bytes 7864320 | tf_op jit(solution)/shard_map/reduce_scatter | solution.py:185
  153.7 0.7 copy-start.8
  153.7 1.1 copy-start.3
  153.8 141.3 %reduce-scatter.3.cloned.1.call-start = ((), (), s32[]{:S(2)}) async-start(), calls=%async_computation.5 | async-start | bytes 1310720 | tf_op jit(solution)/shard_map/reduce_scatter | solution.py:152
  174.8 2.8 copy-start.2
  180.8 0.8 copy-start.1
  184.5 66.4 %copy-start.6 = (f32[128,2]{0,1:T(2,128)S(1)}, f32[128,2]{0,1:T(2,128)}, u32[]{:S(2)}) copy-start(f32[128,2]{0,1:T(2,128)} %param.22) | copy-start | bytes 3076
  243.0 36.6 %all-to-all-start.1 = ((bf16[32,12,2048]{2,1,0:T(8,128)(2,1)}), bf16[32,12,2048]{2,1,0:T(8,128)(2,1)}, u32[]{:S(2)}, u32[]{:S(2)}) async-start(bf16[32,12,2048]{2,1,0:T(8,128)(2,1)} %reshape.124), calls=%async_computation.3 | async-start | bytes 4194304 | tf_op jit(solution)/shard_map/all_to_all | solution.py:193
Sparse Core Ops, SparseCore 0:
  59.2 62.8 all-gather.4
  124.3 50.4 all-gather.2
  177.2 62.0 reduce-scatter.4
  242.2 22.0 reduce-scatter.2

commit v2 on v1

--- a/solution.py
+++ b/solution.py
@@ -125,6 +125,338 @@
     )
 
 
+OFFSETS = (0, 1, 3, 2)
+MESH = pl.DeviceIdType.MESH
+
+
+def arrived(ref, sem):
+    pltpu.make_async_copy(ref, ref, sem).wait()
+
+
+def moe_kernel(
+    out_ref,
+    wg_any,
+    wu_any,
+    wd_any,
+    ret_ref,
+    wg,
+    wu,
+    wd,
+    o4,
+    rx,
+    ys,
+    first,
+    mid,
+    fin,
+    res,
+    r4,
+    xs,
+    hs,
+    w_sem,
+    a2a_send,
+    a2a_recv,
+    ag_send,
+    ag_recv,
+    fw_send,
+    fw_recv,
+    r1_send,
+    r1_recv,
+    rd_send,
+    rm_send,
+    fin_recv,
+    ret_send,
+    ret_recv,
+):
+    me = lax.axis_index("ep")
+    x = lax.axis_index("tp")
+    plane = me // 8
+    place = lax.rem(me, 8)
+    right = lax.rem(x + 1, 4)
+    left = lax.rem(x + 3, 4)
+
+    loads = [
+        pltpu.make_async_copy(src.at[0], dst, w_sem.at[i])
+        for i, (src, dst) in enumerate(((wg_any, wg), (wu_any, wu), (wd_any, wd)))
+    ]
+    for load in loads:
+        load.start()
+
+    barrier = pltpu.get_barrier_semaphore()
+
+    def greet(i, _):
+        pl.semaphore_signal(
+            barrier, inc=1, device_id={"ep": lax.rem(me + i, 32)}, device_id_type=MESH
+        )
+        return 0
+
+    lax.fori_loop(1, 32, greet, 0)
+    for side in (left, right):
+        pl.semaphore_signal(barrier, inc=1, device_id={"tp": side}, device_id_type=MESH)
+
+    def repack(i, _):
+        o4[pl.ds(i * 8, 8)] = out_ref[pl.ds(pl.multiple_of(i * 32, 32), 32), :].reshape(8, 4, 2048)
+        return 0
+
+    lax.fori_loop(0, 12, repack, 0)
+    rx[0, pl.ds(place * 3, 3)] = o4[pl.ds(me * 3, 3)]
+    pl.semaphore_wait(barrier, 33)
+
+    def remote(src, dst, send, recv, device):
+        copy = pltpu.make_async_remote_copy(
+            src_ref=src,
+            dst_ref=dst,
+            send_sem=send,
+            recv_sem=recv,
+            device_id=device,
+            device_id_type=MESH,
+        )
+        copy.start()
+
+    for k, off in enumerate(OFFSETS):
+        far = lax.rem(plane + off, 4) * 8
+
+        def send_rows(i, _, k=k, far=far):
+            j = lax.rem(place + i, 8)
+            remote(
+                o4.at[pl.ds((far + j) * 3, 3)],
+                rx.at[k, pl.ds(place * 3, 3)],
+                a2a_send,
+                a2a_recv.at[k],
+                {"ep": far + j},
+            )
+            return 0
+
+        lax.fori_loop(1 if k == 0 else 0, 8, send_rows, 0)
+
+    def gather_start(k):
+        if k == 0:
+            arrived(rx.at[0, pl.ds(0, 21)], a2a_recv.at[0])
+        else:
+            arrived(rx.at[k, pl.ds(0, 24)], a2a_recv.at[k])
+        own = rx.at[k, pl.ds(0, 24)]
+        remote(own, rx.at[k, pl.ds(24, 24)], ag_send.at[k, 0], ag_recv.at[k, 0], {"tp": right})
+        remote(own, rx.at[k, pl.ds(48, 24)], ag_send.at[k, 1], ag_recv.at[k, 1], {"tp": left})
+
+    def gather_forward(k):
+        arrived(rx.at[k, pl.ds(24, 24)], ag_recv.at[k, 0])
+        remote(
+            rx.at[k, pl.ds(24, 12)],
+            rx.at[k, pl.ds(72, 12)],
+            fw_send.at[k, 0],
+            fw_recv.at[k, 0],
+            {"tp": right},
+        )
+        arrived(rx.at[k, pl.ds(48, 24)], ag_recv.at[k, 1])
+        remote(
+            rx.at[k, pl.ds(60, 12)],
+            rx.at[k, pl.ds(84, 12)],
+            fw_send.at[k, 1],
+            fw_recv.at[k, 1],
+            {"tp": left},
+        )
+
+    def expert(k):
+        if k == 0:
+            for load in loads:
+                load.wait()
+        arrived(rx.at[k, pl.ds(72, 12)], fw_recv.at[k, 0])
+        arrived(rx.at[k, pl.ds(84, 12)], fw_recv.at[k, 1])
+
+        def unpack(i, _):
+            xs[pl.ds(pl.multiple_of(i * 32, 32), 32), :] = rx[k, pl.ds(i * 8, 8)].reshape(32, 2048)
+            return 0
+
+        lax.fori_loop(0, 12, unpack, 0)
+
+        def hidden(at, width):
+            rows = xs[...]
+            gate = jnp.dot(rows, wg[:, pl.ds(at, width)], preferred_element_type=jnp.float32)
+            up = jnp.dot(rows, wu[:, pl.ds(at, width)], preferred_element_type=jnp.float32)
+            hs[:, pl.ds(at, width)] = (gate / (1.0 + jnp.exp(-gate)) * up).astype(jnp.bfloat16)
+
+        def hidden_tile(i, _):
+            hidden(pl.multiple_of(i * 256, 256), 256)
+            return 0
+
+        lax.fori_loop(0, 3, hidden_tile, 0)
+        hidden(768, 128)
+
+        def down(i, _):
+            at = pl.multiple_of(i * 256, 256)
+            part = jnp.dot(hs[...], wd[:, pl.ds(at, 256)], preferred_element_type=jnp.float32)
+            ys[k, :, :, pl.ds(at, 256)] = part.astype(jnp.bfloat16).reshape(96, 4, 256)
+            return 0
+
+        lax.fori_loop(0, 8, down, 0)
+        remote(
+            ys.at[k, pl.ds(72, 12)],
+            first.at[k, 0],
+            r1_send.at[k, 0],
+            r1_recv.at[k, 0],
+            {"tp": right},
+        )
+        remote(
+            ys.at[k, pl.ds(84, 12)],
+            first.at[k, 1],
+            r1_send.at[k, 1],
+            r1_recv.at[k, 1],
+            {"tp": left},
+        )
+        remote(
+            ys.at[k, pl.ds(60, 12)],
+            fin.at[k, 0, pl.ds(12, 12)],
+            rd_send.at[k, 0],
+            fin_recv.at[k, 0],
+            {"tp": right},
+        )
+        remote(
+            ys.at[k, pl.ds(24, 12)],
+            fin.at[k, 1, pl.ds(0, 12)],
+            rd_send.at[k, 1],
+            fin_recv.at[k, 1],
+            {"tp": left},
+        )
+
+    def added(k):
+        for side, at, device in ((0, 48, right), (1, 36, left)):
+            arrived(first.at[k, side], r1_recv.at[k, side])
+
+            def add(i, _, side=side, at=at):
+                both = ys[k, pl.ds(at + i, 1)].astype(jnp.float32) + first[
+                    k, side, pl.ds(i, 1)
+                ].astype(jnp.float32)
+                mid[k, side, pl.ds(i, 1)] = both.astype(jnp.bfloat16)
+                return 0
+
+            lax.fori_loop(0, 12, add, 0)
+            remote(
+                mid.at[k, side],
+                fin.at[k, side, pl.ds(12 * side, 12)],
+                rm_send.at[k, side],
+                fin_recv.at[k, 2 + side],
+                {"tp": device},
+            )
+
+    def back(k):
+        arrived(fin.at[k, 0, pl.ds(12, 12)], fin_recv.at[k, 0])
+        arrived(fin.at[k, 1, pl.ds(0, 12)], fin_recv.at[k, 1])
+        arrived(fin.at[k, 0, pl.ds(0, 12)], fin_recv.at[k, 2])
+        arrived(fin.at[k, 1, pl.ds(12, 12)], fin_recv.at[k, 3])
+
+        def add(i, _):
+            total = ys[k, pl.ds(i, 1)].astype(jnp.float32)
+            total = total + fin[k, 0, pl.ds(i, 1)].astype(jnp.float32)
+            total = total + fin[k, 1, pl.ds(i, 1)].astype(jnp.float32)
+            res[k, pl.ds(i, 1)] = total.astype(jnp.bfloat16)
+            return 0
+
+        lax.fori_loop(0, 24, add, 0)
+        far = lax.rem(plane + 4 - OFFSETS[k], 4) * 8
+
+        def send_back(i, _):
+            j = lax.rem(place + i, 8)
+            remote(
+                res.at[k, pl.ds(j * 3, 3)],
+                r4.at[pl.ds(me * 3, 3)],
+                ret_send,
+                ret_recv,
+                {"ep": far + j},
+            )
+            return 0
+
+        lax.fori_loop(1 if k == 0 else 0, 8, send_back, 0)
+        if k == 0:
+            r4[pl.ds(me * 3, 3)] = res[0, pl.ds(place * 3, 3)]
+
+    gather_start(0)
+    gather_start(1)
+    gather_forward(0)
+    gather_start(2)
+    gather_forward(1)
+    expert(0)
+    gather_start(3)
+    gather_forward(2)
+    expert(1)
+    added(0)
+    gather_forward(3)
+    expert(2)
+    added(1)
+    back(0)
+    expert(3)
+    added(2)
+    back(1)
+    added(3)
+    back(2)
+    back(3)
+
+    arrived(o4.at[pl.ds(0, 93)], a2a_send)
+    for k in range(4):
+        for side in range(2):
+            arrived(rx.at[k, pl.ds(0, 24)], ag_send.at[k, side])
+            arrived(rx.at[k, pl.ds(24, 12)], fw_send.at[k, side])
+            arrived(first.at[k, side], r1_send.at[k, side])
+            arrived(first.at[k, side], rd_send.at[k, side])
+            arrived(first.at[k, side], rm_send.at[k, side])
+    arrived(o4.at[pl.ds(0, 93)], ret_send)
+    arrived(r4.at[pl.ds(0, 93)], ret_recv)
+
+    def unpack_back(i, _):
+        ret_ref[pl.ds(pl.multiple_of(i * 32, 32), 32), :] = r4[pl.ds(i * 8, 8)].reshape(32, 2048)
+        return 0
+
+    lax.fori_loop(0, 12, unpack_back, 0)
+
+
+def experts(outgoing, gate_weight, up_weight, down_weight):
+    rows, width = outgoing.shape
+    ff = gate_weight.shape[2]
+    bf16 = jnp.bfloat16
+    dma = pltpu.SemaphoreType.DMA
+    return pl.pallas_call(
+        moe_kernel,
+        out_shape=jax.ShapeDtypeStruct((rows, width), bf16),
+        in_specs=[pl.BlockSpec(memory_space=pltpu.VMEM)]
+        + [pl.BlockSpec(memory_space=pl.ANY)] * 3,
+        out_specs=pl.BlockSpec(memory_space=pltpu.VMEM),
+        scratch_shapes=[
+            pltpu.VMEM((width, ff), bf16),
+            pltpu.VMEM((width, ff), bf16),
+            pltpu.VMEM((ff, width), bf16),
+            pltpu.VMEM((96, 4, width), bf16),
+            pltpu.VMEM((4, 96, 4, width), bf16),
+            pltpu.VMEM((4, 96, 4, width), bf16),
+            pltpu.VMEM((4, 2, 12, 4, width), bf16),
+            pltpu.VMEM((4, 2, 12, 4, width), bf16),
+            pltpu.VMEM((4, 2, 24, 4, width), bf16),
+            pltpu.VMEM((4, 24, 4, width), bf16),
+            pltpu.VMEM((96, 4, width), bf16),
+            pltpu.VMEM((rows, width), bf16),
+            pltpu.VMEM((rows, ff), bf16),
+            dma((3,)),
+            dma,
+            dma((4,)),
+            dma((4, 2)),
+            dma((4, 2)),
+            dma((4, 2)),
+            dma((4, 2)),
+            dma((4, 2)),
+            dma((4, 2)),
+            dma((4, 2)),
+            dma((4, 2)),
+            dma((4, 4)),
+            dma,
+            dma,
+        ],
+        compiler_params=pltpu.CompilerParams(
+            vmem_limit_bytes=60 * 1024 * 1024, collective_id=0, has_side_effects=True
+        ),
+        cost_estimate=pl.CostEstimate(
+            flops=17_000_000_000, bytes_accessed=14_000_000, transcendentals=1_400_000
+        ),
+        name="experts",
+    )(outgoing, gate_weight, up_weight, down_weight)
+
+
 def body(
     query_rows,
     key_rows,
@@ -174,29 +506,8 @@
     outgoing = (
         jnp.dot(dispatch, normed, preferred_element_type=jnp.float32)
         .astype(jnp.bfloat16)
-        .reshape(expert_count, capacity, model_width)
-    )
-    source_rows = expert_count * capacity
-    arrived = lax.all_to_all(outgoing, "ep", split_axis=0, concat_axis=0, tiled=True)
-    row_piece = lax.all_gather(arrived.reshape(source_rows, model_width), "tp", axis=0, tiled=True)
-    gate_act = jnp.dot(row_piece, gate_weight[0], preferred_element_type=jnp.float32)
-    up_act = jnp.dot(row_piece, up_weight[0], preferred_element_type=jnp.float32)
-    hidden_all = (jax.nn.silu(gate_act) * up_act).astype(jnp.bfloat16)
-    expert_result = lax.psum_scatter(
-        jnp.dot(hidden_all, down_weight[0], preferred_element_type=jnp.float32).astype(
-            jnp.bfloat16
-        ),
-        "tp",
-        scatter_dimension=0,
-        tiled=True,
-    )
-    returned = lax.all_to_all(
-        expert_result.reshape(expert_count, capacity, model_width),
-        "ep",
-        split_axis=0,
-        concat_axis=0,
-        tiled=True,
-    )
+    )
+    returned = experts(outgoing, gate_weight, up_weight, down_weight)
     picked_rows = returned.reshape(-1, model_width)[slot_index.reshape(-1)].reshape(
         tok_count, top_count, model_width
     )

time: 303 us -> 275 us (0.908)
  Pallas kernels: 3.19 us -> 184 us
  waiting for transfers between devices: 157 us -> 41.1 us
  blocking collectives: 38 us -> 0 us
  matrix products: 36.2 us -> 3.52 us
  local copies, waits for them, and re-layouts: 35.9 us -> 22.6 us
  starting transfers between devices: 7.98 us -> 0.08 us
    pallas_call x0 -> x1, Pallas kernels: none -> 181 us  [experts(): pl.pallas_call(moe_kernel, out_shape=jax.ShapeDtypeStruct((rows, width),...]
    all_gather x1 -> x0, waiting for transfers between devices: 61.9 us -> none  [body(): lax.all_gather(arrived.reshape(source_rows, model_width), 'tp', axis=0, t...]
    reduce_scatter x1 -> x0, waiting for transfers between devices: 54.8 us -> none  [body(): lax.psum_scatter(jnp.dot(hidden_all, down_weight[0], preferred_element_ty...]
    all_to_all x1 -> x0, blocking collectives: 38 us -> none  [body(): lax.all_to_all(outgoing, 'ep', split_axis=0, concat_axis=0, tiled=True)]
    dot_general x2 -> x0, matrix products: 31.7 us -> none  [the longest x1 20.3 us: body(): jnp.dot(hidden_all, down_weight[0], preferred_element_type=jnp.float32)]
    all_gather x1, waiting for transfers between devices: 12.1 us -> 41.1 us  [body(): lax.all_gather(augment_kv(key_rows, value_rows, key_bias), 'ep', axis=0,...]
    all_to_all x1 -> x0, waiting for transfers between devices: 28.4 us -> none  [body(): lax.all_to_all(expert_result.reshape(expert_count, capacity, model_width)...]
    reshape x4 -> x0, local copies, waits for them, and re-layouts: 14.5 us -> none  [the longest x1 3.65 us: body(): arrived.reshape(source_rows, model_width)]
  transfers between devices with their start and end apart: 5 -> 2, of which waited for: 4 -> 1; matrix products, arithmetic and copies ran while one was open for 21% -> 9% of each run, Pallas kernels for 1% -> 66%
where the time goes in v2:
time: 275 us; the launch traced here: 274 us
  Pallas kernels  184 us (67%)
  waiting for transfers between devices  41.1 us (15%)
  local copies, waits for them, and re-layouts  22.6 us (8%)
  between operations  14.3 us (5%)
  other arithmetic  8.75 us (3%)
  matrix products  3.52 us (1%)
    pallas_call x1, Pallas kernels, experts(): pl.pallas_call(moe_kernel, out_shape=jax.ShapeDtypeStruct((rows, width),...  181 us
    all_gather x1, waiting for transfers between devices, body(): lax.all_gather(augment_kv(key_rows, value_rows, key_bias), 'ep', axis=0,...  41.1 us
    unnamed x21, local copies, waits for them, and re-layouts  5.6 us
    reduce_sum x1, other arithmetic, body(): jnp.sum(picked_rows.astype(jnp.float32) * route_weight[:, :, None], axis=1)  5.59 us
  transfers between devices with their start and end apart: 2, of which 1 were waited for; matrix products, arithmetic and copies ran while one was open for 9% of the time, Pallas kernels for 66%

profile of v2, /device:TPU:1, one launch (start us, length us, event | category | flops | bytes accessed | tf_op | source)
XLA Modules:
  0.0 274.2 jit_solution(14006431833882886661)
XLA Ops:
  7.2 0.0 copy-start
  7.2 0.0 all-gather.2.cloned.1.call-start
  7.2 0.8 broadcast_multiply_fusion.1
  8.1 0.1 copy.54
  8.2 1.7 concatenate.12
  9.9 0.0 all-gather.2.cloned.1.call-update
  9.9 0.0 reduce-scatter.2.cloned.1.call-start
  10.0 0.8 copy.56
  10.8 0.1 eq.38
  10.9 0.1 eq.42
  11.1 1.1 copy.49
  12.2 0.2 copy.52
  12.4 0.1 stack.21
  12.5 0.1 stack.22
  12.6 0.1 stack.23
  12.7 0.1 copy.53
  12.8 0.9 copy.50
  13.6 0.1 copy.51
  13.7 0.6 reduce-window.6
  14.3 0.2 slice_reduce_fusion
  14.6 0.1 fusion.9
  14.7 0.1 reduce_sum.41
  14.8 0.1 copy.60
  14.9 0.2 mul.68
  15.1 0.7 broadcast_in_dim.41
  16.0 2.2 concatenate.11
  18.2 2.1 concatenate.10
  20.4 1.3 pad_maximum_fusion.q_ref
  21.7 0.2 fusion
  21.9 41.1 %all-gather.2.cloned.1.call-done.kv_ref = bf16[8192,384]{1,0:T(8,128)(2,1)} async-done(((bf16[256,384]{1,0:T(8,128)(2,1)}), bf16[8192,384]{1,0:T(8,128)(2,1)}) %all-gather.2.cloned.1.call-update) | async-done | bytes 6291472 | tf_op jit(solution)/shard_map/all_gather | solution.py:476
  63.0 2.8 %copy-done.2 = bf16[8192,384]{1,0:T(8,128)(2,1)S(1)} copy-done((bf16[8192,384]{1,0:T(8,128)(2,1)S(1)}, bf16[8192,384]{1,0:T(8,128)(2,1)}, u32[]{:S(2)}) %copy-start.2) | copy-done | bytes 6291480
  65.8 3.2 %stick.1 = bf16[2,1024,64]{2,1,0:T(8,128)(2,1)S(1)} custom-call(s32[1]{0:T(128)} %bitcast.count_ref, bf16[2,1024,256]{2,1,0:T(8,128)(2,1)S(1)} %pad_maximum_fusion.q_ref, bf16[8192,384]{1,0:T(8,128)(2,1)S(1)} %copy-done.2), custom_call_target="tpu_custom_call" | custom-call | flops 40000000000 | bytes 8000000 | tf_op jit(solution)/shard_map/stick/pallas_call | solution.py:76
  69.0 0.0 copy-start.1
  69.0 0.8 copy-done.1
  69.8 1.2 copy.55
  71.1 0.0 copy-start.4
  71.1 0.0 copy-start.5
  71.1 1.7 convolution_convert_fusion.1
  72.8 0.0 reduce-scatter.2.cloned.1.call-update
  72.8 0.0 copy-done.4
  72.8 0.0 copy-done.5
  72.8 1.8 convolution_convert_fusion.out_ref
  74.7 180.6 %experts.1 = bf16[384,2048]{1,0:T(8,128)(2,1)} custom-call(bf16[384,2048]{1,0:T(8,128)(2,1)} %convolution_convert_fusion.out_ref, bf16[1,2048,896]{2,1,0:T(8,128)(2,1)} %wg_any.1, bf16[1,2048,896]{2,1,0:T(8,128)(2,1)} %wu_any.1, bf16[1,896,2048]{2,1,0:T(8,128)(2,1)} %wd_any.1), custom_call_target="tpu_custom_call" | custom-call | flops 16999999488 | bytes 14000000 | tf_op jit(solution)/shard_map/experts/pallas_call | solution.py:415
  255.3 4.0 %gather_fusion = bf16[256,2048]{1,0:T(8,128)(2,1)S(1)} fusion(bf16[384,2048]{1,0:T(8,128)(2,1)} %experts.1, s32[1024]{0:T(1024)S(1)} %pad_clamp_fusion), kind=kCustom, calls=%fused_computation | custom fusion | bytes 2098176 | tf_op jit(solution)/shard_map/gather | solution.py:511
  259.3 0.0 copy-start.6
  259.3 2.4 reshape.110
  261.7 0.1 copy.61
  261.8 5.6 %multiply_reduce_fusion = bf16[128,2048]{1,0:T(8,128)(2,1)} fusion(f32[128,2,2048]{2,1,0:T(2,128)} %reshape.110, f32[128,2]{1,0:T(8,128)S(1)} %copy.61), kind=kLoop, calls=%fused_computation.3 | loop fusion | flops 786432 | bytes 2622464 | tf_op jit(solution)/shard_map/reduce_sum | solution.py:514
  (29 shorter events, 0.4 us)
Async XLA Ops:
  7.2 63.9 %copy-start = (bf16[512,2048]{1,0:T(8,128)(2,1)S(1)}, bf16[512,2048]{1,0:T(8,128)(2,1)}, u32[]{:S(2)}) copy-start(bf16[512,2048]{1,0:T(8,128)(2,1)} %param.18) | copy-start | bytes 6291460
  7.2 5.2 %copy-start.7 = (f32[8]{0:T(128)S(1)}, f32[8]{0:T(128)}, u32[]{:S(2)}) copy-start(f32[8]{0:T(128)} %param.17) | copy-start | bytes 100
  7.2 55.9 %all-gather.2.cloned.1.call-start = ((), (), s32[]{:S(2)}) async-start(), calls=%async_computation.1 | async-start | bytes 6488064 | tf_op jit(solution)/shard_map/all_gather | solution.py:476
  9.9 257.4 %reduce-scatter.2.cloned.1.call-start = ((), (), s32[]{:S(2)}) async-start(), calls=%async_computation.2 | async-start | bytes 1310720 | tf_op jit(solution)/shard_map/reduce_scatter | solution.py:484
  20.3 1.4 copy-start.3
  63.0 2.8 %copy-start.2 = (bf16[8192,384]{1,0:T(8,128)(2,1)S(1)}, bf16[8192,384]{1,0:T(8,128)(2,1)}, u32[]{:S(2)}) copy-start(bf16[8192,384]{1,0:T(8,128)(2,1)} %all-gather.2.cloned.1.call-done.kv_ref) | copy-start | bytes 18874372
  69.0 0.8 copy-start.1
  71.1 1.8 copy-start.4
  71.1 1.8 copy-start.5
  259.3 2.4 copy-start.6
Sparse Core Ops, SparseCore 0:
  10.3 52.7 all-gather.1
  73.0 65.2 reduce-scatter.1

commit v3 on v2

v3 whole, which is shorter than its diff:
```python
import math

import jax
import jax.numpy as jnp
from jax import lax
from jax.experimental import pallas as pl
from jax.experimental.pallas import tpu as pltpu
from jax.sharding import PartitionSpec as P

HD = 64
BLK = 256
CAP = 12
EPSILON = 1e-06
TO_LOG2 = math.log2(math.e) / math.sqrt(HD)
OFFSETS = (0, 1, 3, 2)
SEGMENTS = 8
TILE = 512
MESH = pl.DeviceIdType.MESH


def arrived(ref, sem):
    pltpu.make_async_copy(ref, ref, sem).wait()


def remote(src, dst, send, recv, device):
    pltpu.make_async_remote_copy(
        src_ref=src,
        dst_ref=dst,
        send_sem=send,
        recv_sem=recv,
        device_id=device,
        device_id_type=MESH,
    ).start()


def iota(shape, dim):
    return lax.broadcasted_iota(jnp.int32, shape, dim)


def step_kernel(
    query_ref,
    key_ref,
    value_ref,
    bias_ref,
    offset_ref,
    x_ref,
    gain_ref,
    routes_ref,
    rw_ref,
    ow_any,
    wg_any,
    wu_any,
    wd_any,
    mixed_a_ref,
    mixed_b_ref,
    ow,
    wg,
    wu,
    wd,
    o4,
    rx,
    ys,
    first,
    mid,
    fin,
    res,
    r4,
    xs,
    hs,
    kt,
    vv,
    qa,
    acc,
    surv,
    tri,
    ho,
    po,
    pm,
    w_sem,
    a2a_send,
    a2a_recv,
    ag_send,
    ag_recv,
    fw_send,
    fw_recv,
    r1_send,
    r1_recv,
    rd_send,
    rm_send,
    fin_recv,
    ret_send,
    ret_recv,
    ky_send,
    ky_recv,
    kz_send,
    kz_recv,
    kc_send,
    kc_recv,
    po_send,
    po_recv,
):
    me = lax.axis_index("ep")
    x = lax.axis_index("tp")
    plane = me // 8
    place = lax.rem(me, 8)
    row = place // 2
    core = lax.rem(place, 2)
    right = lax.rem(x + 1, 4)
    left = lax.rem(x + 3, 4)
    across = lax.rem(x + 2, 4)
    bf16, f32 = jnp.bfloat16, jnp.float32

    loads = [
        pltpu.make_async_copy(src, dst, w_sem.at[i])
        for i, (src, dst) in enumerate(
            ((wg_any.at[0], wg), (wu_any.at[0], wu), (wd_any.at[0], wd), (ow_any, ow))
        )
    ]
    for load in loads:
        load.start()

    barrier = pltpu.get_barrier_semaphore()

    def greet(i, _):
        pl.semaphore_signal(
            barrier, inc=1, device_id={"ep": lax.rem(me + i, 32)}, device_id_type=MESH
        )
        return 0

    lax.fori_loop(1, 32, greet, 0)
    for side in (left, right, across):
        pl.semaphore_signal(barrier, inc=1, device_id={"tp": side}, device_id_type=MESH)

    def clear(i, _):
        kt[i, pl.ds(144, 112), :] = jnp.zeros((112, BLK), bf16)
        return 0

    lax.fori_loop(0, 32, clear, 0)
    own = plane * 8 + core * 4 + row
    kt[own, pl.ds(0, 128), :] = key_ref[...].astype(f32).T.astype(bf16)
    bias = bias_ref[...].astype(f32) * 8.0
    sub = iota((16, BLK), 0)
    extra = jnp.where(sub == 0, bias[0:1, :], jnp.where(sub == 1, bias[1:2, :], 0.0))
    extra = jnp.where((sub >= 2) & (sub <= 4), 1.0, extra)
    kt[own, pl.ds(128, 16), :] = extra.astype(bf16)
    vv[own, :, pl.ds(0, 128)] = value_ref[pl.ds(0, 128), :]
    vv[own, :, pl.ds(128, 128)] = value_ref[pl.ds(128, 128), :]

    expert_at = iota((32, 128), 0)
    earlier = jnp.where(iota((128, 128), 0) < iota((128, 128), 1), 1.0, 0.0).astype(bf16)
    base = (expert_at * CAP).astype(f32)
    slots = []
    for c in range(2):
        named = expert_at == routes_ref[c : c + 1, :]
        count = jnp.where(named, 1.0, 0.0)
        rank = base + jnp.dot(count.astype(bf16), earlier, preferred_element_type=f32)
        slots.append(jnp.sum(jnp.where(named, rank, 0.0), axis=0, keepdims=True).astype(jnp.int32))
        base = base + jnp.sum(count, axis=1, keepdims=True)
    slot_at = iota((32 * CAP, 128), 0)

    def norm(i, _):
        at = pl.ds(pl.multiple_of(i * 32, 32), 32)
        values = x_ref[at, :].astype(f32)
        scale = lax.rsqrt(jnp.mean(values * values, axis=1, keepdims=True) + EPSILON)
        xs[at, :] = (values * scale * gain_ref[...]).astype(bf16)
        return 0

    lax.fori_loop(0, 4, norm, 0)
    pick = jnp.where((slot_at == slots[0]) | (slot_at == slots[1]), 1.0, 0.0).astype(bf16)

    def dispatch(i, _):
        at = pl.ds(pl.multiple_of(i * 256, 256), 256)
        rows = jnp.dot(pick, xs[pl.ds(0, 128), at], preferred_element_type=f32)
        o4[:, :, at] = rows.astype(bf16).reshape(96, 4, 256)
        return 0

    lax.fori_loop(0, 8, dispatch, 0)
    rx[0, pl.ds(place * 3, 3)] = o4[pl.ds(me * 3, 3)]
    pl.semaphore_wait(barrier, 34)

    def along_y(d):
        return {"ep": plane * 8 + lax.rem(row + d, 4) * 2 + core}

    def along_z(d):
        return {"ep": lax.rem(plane + d, 4) * 8 + place}

    def kt_y(d):
        return kt.at[plane * 8 + core * 4 + lax.rem(row + d, 4), pl.ds(0, 144)]

    def vv_y(d):
        return vv.at[plane * 8 + core * 4 + lax.rem(row + d, 4)]

    def kt_z(d, c=core):
        return kt.at[pl.ds(lax.rem(plane + d, 4) * 8 + c * 4, 4), pl.ds(0, 144)]

    def vv_z(d, c=core):
        return vv.at[pl.ds(lax.rem(plane + d, 4) * 8 + c * 4, 4)]

    def keys_y():
        for s, d in enumerate((1, 3)):
            remote(kt_y(0), kt_y(0), ky_send.at[s, 0], ky_recv.at[s, 0], along_y(d))
            remote(vv_y(0), vv_y(0), ky_send.at[s, 1], ky_recv.at[s, 1], along_y(d))

    def keys_y_on():
        arrived(kt_y(3), ky_recv.at[0, 0])
        remote(kt_y(3), kt_y(3), ky_send.at[2, 0], ky_recv.at[2, 0], along_y(1))
        arrived(vv_y(1), ky_recv.at[1, 1])
        remote(vv_y(1), vv_y(1), ky_send.at[2, 1], ky_recv.at[2, 1], along_y(3))
        arrived(vv_y(3), ky_recv.at[0, 1])
        arrived(kt_y(1), ky_recv.at[1, 0])

    def keys_z():
        arrived(kt_y(2), ky_recv.at[2, 0])
        arrived(vv_y(2), ky_recv.at[2, 1])
        for s, d in enumerate((1, 3)):
            remote(kt_z(0), kt_z(0), kz_send.at[s, 0], kz_recv.at[s, 0], along_z(d))
            remote(vv_z(0), vv_z(0), kz_send.at[s, 1], kz_recv.at[s, 1], along_z(d))

    def keys_z_on():
        arrived(kt_z(3), kz_recv.at[0, 0])
        remote(kt_z(3), kt_z(3), kz_send.at[2, 0], kz_recv.at[2, 0], along_z(1))
        arrived(vv_z(1), kz_recv.at[1, 1])
        remote(vv_z(1), vv_z(1), kz_send.at[2, 1], kz_recv.at[2, 1], along_z(3))
        arrived(vv_z(3), kz_recv.at[0, 1])
        arrived(kt_z(1), kz_recv.at[1, 0])

    def keys_core():
        arrived(kt_z(2), kz_recv.at[2, 0])
        arrived(vv_z(2), kz_recv.at[2, 1])
        for d in range(4):
            device = {"ep": me + 1 - 2 * core}
            remote(kt_z(d), kt_z(d), kc_send.at[d, 0], kc_recv.at[d, 0], device)
            remote(vv_z(d), vv_z(d), kc_send.at[d, 1], kc_recv.at[d, 1], device)

    def keys_here():
        for d in range(4):
            arrived(kt_z(d, 1 - core), kc_recv.at[d, 0])
            arrived(vv_z(d, 1 - core), kc_recv.at[d, 1])

    keys_y()

    for k, off in enumerate(OFFSETS):
        far = lax.rem(plane + off, 4) * 8

        def send_rows(i, _, k=k, far=far):
            j = lax.rem(place + i, 8)
            remote(
                o4.at[pl.ds((far + j) * 3, 3)],
                rx.at[k, pl.ds(place * 3, 3)],
                a2a_send,
                a2a_recv.at[k],
                {"ep": far + j},
            )
            return 0

        lax.fori_loop(1 if k == 0 else 0, 8, send_rows, 0)

    def gather_start(k):
        if k == 0:
            arrived(rx.at[0, pl.ds(0, 21)], a2a_recv.at[0])
        else:
            arrived(rx.at[k, pl.ds(0, 24)], a2a_recv.at[k])
        own = rx.at[k, pl.ds(0, 24)]
        remote(own, rx.at[k, pl.ds(24, 24)], ag_send.at[k, 0], ag_recv.at[k, 0], {"tp": right})
        remote(own, rx.at[k, pl.ds(48, 24)], ag_send.at[k, 1], ag_recv.at[k, 1], {"tp": left})

    def gather_forward(k):
        arrived(rx.at[k, pl.ds(24, 24)], ag_recv.at[k, 0])
        remote(
            rx.at[k, pl.ds(24, 12)],
            rx.at[k, pl.ds(72, 12)],
            fw_send.at[k, 0],
            fw_recv.at[k, 0],
            {"tp": right},
        )
        arrived(rx.at[k, pl.ds(48, 24)], ag_recv.at[k, 1])
        remote(
            rx.at[k, pl.ds(60, 12)],
            rx.at[k, pl.ds(84, 12)],
            fw_send.at[k, 1],
            fw_recv.at[k, 1],
            {"tp": left},
        )

    def expert(k):
        if k == 0:
            for load in loads[:3]:
                load.wait()
        arrived(rx.at[k, pl.ds(72, 12)], fw_recv.at[k, 0])
        arrived(rx.at[k, pl.ds(84, 12)], fw_recv.at[k, 1])

        def unpack(i, _):
            xs[pl.ds(pl.multiple_of(i * 32, 32), 32), :] = rx[k, pl.ds(i * 8, 8)].reshape(32, 2048)
            return 0

        lax.fori_loop(0, 12, unpack, 0)

        def hidden(at, width):
            rows = xs[...]
            gate = jnp.dot(rows, wg[:, pl.ds(at, width)], preferred_element_type=jnp.float32)
            up = jnp.dot(rows, wu[:, pl.ds(at, width)], preferred_element_type=jnp.float32)
            hs[:, pl.ds(at, width)] = (gate / (1.0 + jnp.exp(-gate)) * up).astype(jnp.bfloat16)

        def hidden_tile(i, _):
            hidden(pl.multiple_of(i * 256, 256), 256)
            return 0

        lax.fori_loop(0, 3, hidden_tile, 0)
        hidden(768, 128)

        def down(i, _):
            at = pl.multiple_of(i * 256, 256)
            part = jnp.dot(hs[...], wd[:, pl.ds(at, 256)], preferred_element_type=jnp.float32)
            ys[k, :, :, pl.ds(at, 256)] = part.astype(jnp.bfloat16).reshape(96, 4, 256)
            return 0

        lax.fori_loop(0, 8, down, 0)
        remote(
            ys.at[k, pl.ds(72, 12)],
            first.at[k, 0],
            r1_send.at[k, 0],
            r1_recv.at[k, 0],
            {"tp": right},
        )
        remote(
            ys.at[k, pl.ds(84, 12)],
            first.at[k, 1],
            r1_send.at[k, 1],
            r1_recv.at[k, 1],
            {"tp": left},
        )
        remote(
            ys.at[k, pl.ds(60, 12)],
            fin.at[k, 0, pl.ds(12, 12)],
            rd_send.at[k, 0],
            fin_recv.at[k, 0],
            {"tp": right},
        )
        remote(
            ys.at[k, pl.ds(24, 12)],
            fin.at[k, 1, pl.ds(0, 12)],
            rd_send.at[k, 1],
            fin_recv.at[k, 1],
            {"tp": left},
        )

    def added(k):
        for side, at, device in ((0, 48, right), (1, 36, left)):
            arrived(first.at[k, side], r1_recv.at[k, side])

            def add(i, _, side=side, at=at):
                both = ys[k, pl.ds(at + i, 1)].astype(jnp.float32) + first[
                    k, side, pl.ds(i, 1)
                ].astype(jnp.float32)
                mid[k, side, pl.ds(i, 1)] = both.astype(jnp.bfloat16)
                return 0

            lax.fori_loop(0, 12, add, 0)
            remote(
                mid.at[k, side],
                fin.at[k, side, pl.ds(12 * side, 12)],
                rm_send.at[k, side],
                fin_recv.at[k, 2 + side],
                {"tp": device},
            )

    def back(k):
        arrived(fin.at[k, 0, pl.ds(12, 12)], fin_recv.at[k, 0])
        arrived(fin.at[k, 1, pl.ds(0, 12)], fin_recv.at[k, 1])
        arrived(fin.at[k, 0, pl.ds(0, 12)], fin_recv.at[k, 2])
        arrived(fin.at[k, 1, pl.ds(12, 12)], fin_recv.at[k, 3])

        def add(i, _):
            total = ys[k, pl.ds(i, 1)].astype(jnp.float32)
            total = total + fin[k, 0, pl.ds(i, 1)].astype(jnp.float32)
            total = total + fin[k, 1, pl.ds(i, 1)].astype(jnp.float32)
            res[k, pl.ds(i, 1)] = total.astype(jnp.bfloat16)
            return 0

        lax.fori_loop(0, 24, add, 0)
        far = lax.rem(plane + 4 - OFFSETS[k], 4) * 8

        def send_back(i, _):
            j = lax.rem(place + i, 8)
            remote(
                res.at[k, pl.ds(j * 3, 3)],
                r4.at[pl.ds(me * 3, 3)],
                ret_send,
                ret_recv,
                {"ep": far + j},
            )
            return 0

        lax.fori_loop(1 if k == 0 else 0, 8, send_back, 0)
        if k == 0:
            r4[pl.ds(me * 3, 3)] = res[0, pl.ds(place * 3, 3)]

    def queries():
        lane = iota((1, 128), 1)
        half = iota((BLK, 128), 1) < HD
        for g in range(2):
            for j in range(4):
                h = 4 * g + j
                pair = query_ref[:, 128 * (h // 2) : 128 * (h // 2 + 1)].astype(f32)
                if h % 2 != g:
                    pair = pltpu.roll(pair, HD, 1)
                qa[g, pl.ds(BLK * j, BLK), pl.ds(0, 128)] = jnp.where(
                    half if g == 0 else ~half, pair, 0.0
                ).astype(bf16)
                rest = jnp.full((1, 128), offset_ref[h] * 8.0, f32)
                columns = jnp.where(lane == g, 1.0, 0.0)
                for t in range(3):
                    term = rest.astype(bf16).astype(f32)
                    columns = jnp.where(lane == 2 + t, term, columns)
                    rest = rest - term
                qa[g, pl.ds(BLK * j, BLK), pl.ds(128, 128)] = jnp.broadcast_to(
                    columns, (BLK, 128)
                ).astype(bf16)
        tri[...] = jnp.where(iota((BLK, BLK), 0) > iota((BLK, BLK), 1), -1.0, 0.0).astype(bf16)
        acc[...] = jnp.zeros_like(acc)
        surv[...] = jnp.zeros_like(surv)

    def block(index, diagonal):
        at = (index // 8) * 8 + lax.rem(index, 2) * 4 + lax.rem(index, 8) // 2
        keys = kt[at]
        for g in range(2):
            vals = jnp.concatenate(
                [
                    vv[at, :, HD * g : HD * (g + 1)],
                    vv[at, :, 128 + HD * g : 128 + HD * (g + 1)],
                ],
                axis=0,
            )
            for m in range(4 * BLK // TILE):
                part = slice(m * TILE, (m + 1) * TILE)
                z = jnp.dot(qa[g, part, :], keys, preferred_element_type=f32) * TO_LOG2
                if diagonal:
                    z = jnp.where(
                        iota((TILE, BLK), 1) < lax.rem(iota((TILE, BLK), 0), BLK), z, -1e30
                    )
                leave = jnp.maximum(z, jnp.log2(1.0 + jnp.exp2(jnp.minimum(z, 100.0))))
                after = jnp.dot(leave.astype(bf16), tri[...], preferred_element_type=f32) - leave
                s = surv[g, part, :]
                w = jnp.exp2(z + after + jnp.concatenate([s, s], axis=1)).astype(bf16)
                acc[g, part, :] += jnp.dot(w, vals, preferred_element_type=f32)
                surv[g, part, :] = s + jnp.broadcast_to(after[:, 0:1], s.shape)

    def attend(first_part, last_part):
        def step(i, _):
            block(me - 1 - i, False)
            return 0

        lax.fori_loop(me * first_part // SEGMENTS, me * last_part // SEGMENTS, step, 0)

    def project():
        for h in range(0, 8, 2):
            pair = [
                acc[(h + i) // 4, pl.ds(BLK * ((h + i) % 4), BLK), :].astype(bf16)
                for i in range(2)
            ]
            ho[:, pl.ds(HD * h, 2 * HD)] = jnp.concatenate(pair, axis=1)
        loads[3].wait()

        def out(i, _):
            at = pl.ds(pl.multiple_of(i * 256, 256), 256)
            part = jnp.dot(ho[...], ow[:, at], preferred_element_type=f32).astype(bf16)
            po[:, :, at] = part.reshape(4, 64, 256)
            return 0

        lax.fori_loop(0, 8, out, 0)
        for s, side in enumerate((across, right, left)):
            remote(po.at[side], pm.at[s], po_send.at[s], po_recv.at[s], {"tp": side})

    def mixed():
        for s in range(3):
            arrived(pm.at[s], po_recv.at[s])
        total = po[x].astype(f32)
        for s in range(3):
            total = total + pm[s].astype(f32)
        mixed_a_ref[...] = total.astype(bf16)

    gather_start(0)
    keys_y_on()
    gather_start(1)
    keys_z()
    gather_start(2)
    gather_forward(0)
    queries()
    keys_z_on()
    gather_start(3)
    gather_forward(1)
    keys_core()
    expert(0)
    gather_forward(2)
    expert(1)
    added(0)
    gather_forward(3)
    expert(2)
    added(1)
    back(0)
    expert(3)
    added(2)
    keys_here()
    block(me, True)
    attend(0, 1)
    added(3)
    back(1)
    attend(1, 3)
    back(2)
    attend(3, 5)
    back(3)
    attend(5, SEGMENTS)
    project()

    arrived(o4.at[pl.ds(0, 93)], a2a_send)
    for k in range(4):
        for side in range(2):
            arrived(rx.at[k, pl.ds(0, 24)], ag_send.at[k, side])
            arrived(rx.at[k, pl.ds(24, 12)], fw_send.at[k, side])
            arrived(first.at[k, side], r1_send.at[k, side])
            arrived(first.at[k, side], rd_send.at[k, side])
            arrived(first.at[k, side], rm_send.at[k, side])
    for s in range(3):
        arrived(kt_y(0), ky_send.at[s, 0])
        arrived(vv_y(0), ky_send.at[s, 1])
        arrived(kt_z(0), kz_send.at[s, 0])
        arrived(vv_z(0), kz_send.at[s, 1])
    for d in range(4):
        arrived(kt_z(0), kc_send.at[d, 0])
        arrived(vv_z(0), kc_send.at[d, 1])
    arrived(o4.at[pl.ds(0, 93)], ret_send)
    arrived(r4.at[pl.ds(0, 93)], ret_recv)

    def unpack_back(i, _):
        xs[pl.ds(pl.multiple_of(i * 32, 32), 32), :] = r4[pl.ds(i * 8, 8)].reshape(32, 2048)
        return 0

    lax.fori_loop(0, 12, unpack_back, 0)
    weight = jnp.where(slot_at == slots[0], rw_ref[0:1, :], 0.0)
    weight = weight + jnp.where(slot_at == slots[1], rw_ref[1:2, :], 0.0)
    high = weight.astype(bf16)
    low = (weight - high.astype(f32)).astype(bf16)

    def combine(i, _):
        at = pl.ds(pl.multiple_of(i * 256, 256), 256)
        rows = xs[:, at]
        dims = (((0,), (0,)), ((), ()))
        total = lax.dot_general(high, rows, dims, preferred_element_type=f32)
        total = total + lax.dot_general(low, rows, dims, preferred_element_type=f32)
        mixed_b_ref[:, at] = total.astype(bf16)
        return 0

    lax.fori_loop(0, 8, combine, 0)
    mixed()
    for s in range(3):
        arrived(pm.at[s], po_send.at[s])


def body(
    query_rows,
    key_rows,
    value_rows,
    key_bias,
    head_offset,
    out_weight,
    expert_input,
    expert_gain,
    routes,
    route_weight,
    gate_weight,
    up_weight,
    down_weight,
):
    width, ff = gate_weight.shape[1:]
    tokens = expert_input.shape[0]
    rows = 32 * CAP
    bf16, f32 = jnp.bfloat16, jnp.float32
    dma = pltpu.SemaphoreType.DMA
    vmem = pltpu.VMEM
    here, there = pl.BlockSpec(memory_space=vmem), pl.BlockSpec(memory_space=pl.ANY)
    return pl.pallas_call(
        step_kernel,
        out_shape=(
            jax.ShapeDtypeStruct((BLK // 4, width), bf16),
            jax.ShapeDtypeStruct((tokens, width), bf16),
        ),
        in_specs=[here] * 4
        + [pl.BlockSpec(memory_space=pltpu.SMEM)]
        + [here] * 4
        + [there] * 4,
        out_specs=(here, here),
        scratch_shapes=[
            vmem((8 * HD, width), bf16),
            vmem((width, ff), bf16),
            vmem((width, ff), bf16),
            vmem((ff, width), bf16),
            vmem((96, 4, width), bf16),
            vmem((4, 96, 4, width), bf16),
            vmem((4, 96, 4, width), bf16),
            vmem((4, 2, 12, 4, width), bf16),
            vmem((4, 2, 12, 4, width), bf16),
            vmem((4, 2, 24, 4, width), bf16),
            vmem((4, 24, 4, width), bf16),
            vmem((96, 4, width), bf16),
            vmem((rows, width), bf16),
            vmem((rows, ff), bf16),
            vmem((32, BLK, BLK), bf16),
            vmem((32, BLK // 2, BLK), bf16),
            vmem((2, 4 * BLK, 256), bf16),
            vmem((2, 4 * BLK, HD), f32),
            vmem((2, 4 * BLK, 128), f32),
            vmem((BLK, BLK), bf16),
            vmem((BLK, 8 * HD), bf16),
            vmem((4, BLK // 4, width), bf16),
            vmem((3, BLK // 4, width), bf16),
            dma((4,)),
            dma,
            dma((4,)),
            dma((4, 2)),
            dma((4, 2)),
            dma((4, 2)),
            dma((4, 2)),
            dma((4, 2)),
            dma((4, 2)),
            dma((4, 2)),
            dma((4, 2)),
            dma((4, 4)),
            dma,
            dma,
            dma((3, 2)),
            dma((3, 2)),
            dma((3, 2)),
            dma((3, 2)),
            dma((4, 2)),
            dma((4, 2)),
            dma((3,)),
            dma((3,)),
        ],
        compiler_params=pltpu.CompilerParams(
            vmem_limit_bytes=63 * 1024 * 1024, collective_id=0, has_side_effects=True
        ),
        name="step",
    )(
        query_rows,
        key_rows,
        value_rows,
        key_bias.T,
        head_offset,
        expert_input,
        expert_gain[None, :],
        routes.T,
        route_weight.T,
        out_weight,
        gate_weight,
        up_weight,
        down_weight,
    )


def solution(mesh):
    return jax.shard_map(
        body,
        mesh=mesh,
        in_specs=(
            P("ep", "tp"),
            P("ep", "tp"),
            P("ep", "tp"),
            P("ep", "tp"),
            P("tp"),
            P("tp", None),
            P(("ep", "tp"), None),
            P(),
            P(("ep", "tp"), None),
            P(("ep", "tp"), None),
            P("ep", None, "tp"),
            P("ep", None, "tp"),
            P("ep", "tp", None),
        ),
        out_specs=(P(("ep", "tp"), None), P(("ep", "tp"), None)),
        check_vma=False,
    )
```

time: 275 us -> 167 us (0.61)
  the two profiles are of different devices: /device:TPU:1 before, /device:TPU:120 now
where the time goes in v3:
time: 167 us
  Pallas kernels  163 us (98%)
  local copies, waits for them, and re-layouts  3.55 us (2%)
    pallas_call x1, Pallas kernels, body(): pl.pallas_call(step_kernel, out_shape=(jax.ShapeDtypeStruct((BLK // 4, wi...  163 us
    unnamed x2, local copies, waits for them, and re-layouts  3.55 us

profile of v3, /device:TPU:120, one launch (start us, length us, event | category | flops | bytes accessed | tf_op | source)
XLA Modules:
  0.0 167.0 jit_solution(3584989029434495169)
XLA Ops:
  0.6 162.8 %step.1 = (bf16[64,2048]{1,0:T(8,128)(2,1)}, bf16[128,2048]{1,0:T(8,128)(2,1)}) custom-call(bf16[256,512]{1,0:T(8,128)(2,1)} %query_ref.1, bf16[256,128]{1,0:T(8,128)(2,1)} %key_ref.1, bf16[256,128]{1,0:T(8,128)(2,1)} %value_ref.1, bf16[2,256]{1,0:T(2,128)(2,1)} %bitcast.5, f32[8]{0:T(128)} %offset_ref.1, bf16[128,2048]{1,0:T(8,128)(2,1)} %x_ref.1, ...), custom_call_target="tpu_custom_call" | custom-call | tf_op jit(solution)/shard_map/step/pallas_call | solution.py:581
  163.5 1.7 copy.17
  165.2 1.9 %copy.18 = bf16[128,2048]{1,0:T(8,128)(2,1)} copy(bf16[128,2048]{1,0:T(8,128)(2,1)} %get-tuple-element.5) | data formatting | bytes 1048576

commit v4 on v3

--- a/solution.py
+++ b/solution.py
@@ -13,7 +13,7 @@
 EPSILON = 1e-06
 TO_LOG2 = math.log2(math.e) / math.sqrt(HD)
 OFFSETS = (0, 1, 3, 2)
-SEGMENTS = 8
+SHARE = 16
 TILE = 512
 MESH = pl.DeviceIdType.MESH
 
@@ -98,6 +98,11 @@
     kc_recv,
     po_send,
     po_recv,
+    guest,
+    far_out,
+    far_in,
+    pair_send,
+    pair_recv,
 ):
     me = lax.axis_index("ep")
     x = lax.axis_index("tp")
@@ -108,6 +113,9 @@
     right = lax.rem(x + 1, 4)
     left = lax.rem(x + 3, 4)
     across = lax.rem(x + 2, 4)
+    partner = {"ep": 31 - me}
+    guests = jnp.maximum(SHARE - 1 - me, 0)
+    near = jnp.minimum(me, SHARE)
     bf16, f32 = jnp.bfloat16, jnp.float32
 
     loads = [
@@ -237,8 +245,6 @@
             arrived(kt_z(d, 1 - core), kc_recv.at[d, 0])
             arrived(vv_z(d, 1 - core), kc_recv.at[d, 1])
 
-    keys_y()
-
     for k, off in enumerate(OFFSETS):
         far = lax.rem(plane + off, 4) * 8
 
@@ -255,6 +261,12 @@
 
         lax.fori_loop(1 if k == 0 else 0, 8, send_rows, 0)
 
+    keys_y()
+
+    @pl.when(me >= SHARE)
+    def _():
+        remote(query_ref, guest, pair_send.at[0], pair_recv.at[0], partner)
+
     def gather_start(k):
         if k == 0:
             arrived(rx.at[0, pl.ds(0, 21)], a2a_recv.at[0])
@@ -349,13 +361,13 @@
             arrived(first.at[k, side], r1_recv.at[k, side])
 
             def add(i, _, side=side, at=at):
-                both = ys[k, pl.ds(at + i, 1)].astype(jnp.float32) + first[
-                    k, side, pl.ds(i, 1)
+                both = ys[k, pl.ds(at + 2 * i, 2)].astype(jnp.float32) + first[
+                    k, side, pl.ds(2 * i, 2)
                 ].astype(jnp.float32)
-                mid[k, side, pl.ds(i, 1)] = both.astype(jnp.bfloat16)
+                mid[k, side, pl.ds(2 * i, 2)] = both.astype(jnp.bfloat16)
                 return 0
 
-            lax.fori_loop(0, 12, add, 0)
+            lax.fori_loop(0, 6, add, 0)
             remote(
                 mid.at[k, side],
                 fin.at[k, side, pl.ds(12 * side, 12)],
@@ -371,13 +383,13 @@
         arrived(fin.at[k, 1, pl.ds(12, 12)], fin_recv.at[k, 3])
 
         def add(i, _):
-            total = ys[k, pl.ds(i, 1)].astype(jnp.float32)
-            total = total + fin[k, 0, pl.ds(i, 1)].astype(jnp.float32)
-            total = total + fin[k, 1, pl.ds(i, 1)].astype(jnp.float32)
-            res[k, pl.ds(i, 1)] = total.astype(jnp.bfloat16)
-            return 0
-
-        lax.fori_loop(0, 24, add, 0)
+            total = ys[k, pl.ds(2 * i, 2)].astype(jnp.float32)
+            total = total + fin[k, 0, pl.ds(2 * i, 2)].astype(jnp.float32)
+            total = total + fin[k, 1, pl.ds(2 * i, 2)].astype(jnp.float32)
+            res[k, pl.ds(2 * i, 2)] = total.astype(jnp.bfloat16)
+            return 0
+
+        lax.fori_loop(0, 12, add, 0)
         far = lax.rem(plane + 4 - OFFSETS[k], 4) * 8
 
         def send_back(i, _):
@@ -386,7 +398,7 @@
                 res.at[k, pl.ds(j * 3, 3)],
                 r4.at[pl.ds(me * 3, 3)],
                 ret_send,
-                ret_recv,
+                ret_recv.at[k],
                 {"ep": far + j},
             )
             return 0
@@ -395,13 +407,13 @@
         if k == 0:
             r4[pl.ds(me * 3, 3)] = res[0, pl.ds(place * 3, 3)]
 
-    def queries():
+    def queries(source):
         lane = iota((1, 128), 1)
         half = iota((BLK, 128), 1) < HD
         for g in range(2):
             for j in range(4):
                 h = 4 * g + j
-                pair = query_ref[:, 128 * (h // 2) : 128 * (h // 2 + 1)].astype(f32)
+                pair = source[:, 128 * (h // 2) : 128 * (h // 2 + 1)].astype(f32)
                 if h % 2 != g:
                     pair = pltpu.roll(pair, HD, 1)
                 qa[g, pl.ds(BLK * j, BLK), pl.ds(0, 128)] = jnp.where(
@@ -416,7 +428,6 @@
                 qa[g, pl.ds(BLK * j, BLK), pl.ds(128, 128)] = jnp.broadcast_to(
                     columns, (BLK, 128)
                 ).astype(bf16)
-        tri[...] = jnp.where(iota((BLK, BLK), 0) > iota((BLK, BLK), 1), -1.0, 0.0).astype(bf16)
         acc[...] = jnp.zeros_like(acc)
         surv[...] = jnp.zeros_like(surv)
 
@@ -445,14 +456,47 @@
                 acc[g, part, :] += jnp.dot(w, vals, preferred_element_type=f32)
                 surv[g, part, :] = s + jnp.broadcast_to(after[:, 0:1], s.shape)
 
-    def attend(first_part, last_part):
+    def attend_start():
+        tri[...] = jnp.where(iota((BLK, BLK), 0) > iota((BLK, BLK), 1), -1.0, 0.0).astype(bf16)
+
+        @pl.when(me < SHARE)
+        def _():
+            arrived(guest, pair_recv.at[0])
+            queries(guest)
+
+    def own_start():
+        @pl.when(me < SHARE)
+        def _():
+            far_out[...] = jnp.concatenate([acc[0], acc[1]], axis=1).astype(bf16)
+            remote(far_out, far_in, pair_send.at[1], pair_recv.at[1], partner)
+
+        queries(query_ref)
+        block(me, True)
+
+    def attend(begin, end):
         def step(i, _):
-            block(me - 1 - i, False)
-            return 0
-
-        lax.fori_loop(me * first_part // SEGMENTS, me * last_part // SEGMENTS, step, 0)
+            @pl.when(i == guests)
+            def _():
+                own_start()
+
+            @pl.when(i != guests)
+            def _():
+                block(jnp.where(i < guests, SHARE - 2 - me - i, me + guests - i), False)
+
+            return 0
+
+        lax.fori_loop(
+            jnp.minimum(begin, guests + 1 + near), jnp.minimum(end, guests + 1 + near), step, 0
+        )
 
     def project():
+        @pl.when(me >= SHARE)
+        def _():
+            arrived(far_in, pair_recv.at[1])
+            for g in range(2):
+                far = far_in[:, HD * g : HD * (g + 1)].astype(f32)
+                acc[g] += jnp.exp2(surv[g, :, 0:HD]) * far
+
         for h in range(0, 8, 2):
             pair = [
                 acc[(h + i) // 4, pl.ds(BLK * ((h + i) % 4), BLK), :].astype(bf16)
@@ -480,17 +524,16 @@
         mixed_a_ref[...] = total.astype(bf16)
 
     gather_start(0)
+    gather_start(1)
     keys_y_on()
-    gather_start(1)
-    keys_z()
     gather_start(2)
     gather_forward(0)
-    queries()
-    keys_z_on()
+    keys_z()
     gather_start(3)
     gather_forward(1)
+    keys_z_on()
+    expert(0)
     keys_core()
-    expert(0)
     gather_forward(2)
     expert(1)
     added(0)
@@ -501,15 +544,16 @@
     expert(3)
     added(2)
     keys_here()
-    block(me, True)
-    attend(0, 1)
+    attend_start()
+    attend(0, 4)
     added(3)
+    attend(4, 8)
     back(1)
-    attend(1, 3)
+    attend(8, 13)
     back(2)
-    attend(3, 5)
+    attend(13, 15)
     back(3)
-    attend(5, SEGMENTS)
+    attend(15, 17)
     project()
 
     arrived(o4.at[pl.ds(0, 93)], a2a_send)
@@ -529,13 +573,18 @@
         arrived(kt_z(0), kc_send.at[d, 0])
         arrived(vv_z(0), kc_send.at[d, 1])
     arrived(o4.at[pl.ds(0, 93)], ret_send)
-    arrived(r4.at[pl.ds(0, 93)], ret_recv)
-
-    def unpack_back(i, _):
-        xs[pl.ds(pl.multiple_of(i * 32, 32), 32), :] = r4[pl.ds(i * 8, 8)].reshape(32, 2048)
-        return 0
-
-    lax.fori_loop(0, 12, unpack_back, 0)
+
+    for k in range(4):
+        arrived(r4.at[pl.ds(0, 21 if k == 0 else 24)], ret_recv.at[k])
+        far = lax.rem(plane + OFFSETS[k], 4) * 24
+
+        def unpack_back(i, _, far=far):
+            at = far + i * 8
+            xs[pl.ds(pl.multiple_of(at * 4, 32), 32), :] = r4[pl.ds(at, 8)].reshape(32, 2048)
+            return 0
+
+        lax.fori_loop(0, 3, unpack_back, 0)
+
     weight = jnp.where(slot_at == slots[0], rw_ref[0:1, :], 0.0)
     weight = weight + jnp.where(slot_at == slots[1], rw_ref[1:2, :], 0.0)
     high = weight.astype(bf16)
@@ -554,6 +603,14 @@
     mixed()
     for s in range(3):
         arrived(pm.at[s], po_send.at[s])
+
+    @pl.when(me >= SHARE)
+    def _():
+        arrived(guest, pair_send.at[0])
+
+    @pl.when(me < SHARE)
+    def _():
+        arrived(far_in, pair_send.at[1])
 
 
 def body(
@@ -626,7 +683,7 @@
             dma((4, 2)),
             dma((4, 4)),
             dma,
-            dma,
+            dma((4,)),
             dma((3, 2)),
             dma((3, 2)),
             dma((3, 2)),
@@ -635,6 +692,11 @@
             dma((4, 2)),
             dma((3,)),
             dma((3,)),
+            vmem((BLK, 8 * HD), bf16),
+            vmem((4 * BLK, 2 * HD), bf16),
+            vmem((4 * BLK, 2 * HD), bf16),
+            dma((2,)),
+            dma((2,)),
         ],
         compiler_params=pltpu.CompilerParams(
             vmem_limit_bytes=63 * 1024 * 1024, collective_id=0, has_side_effects=True

time: 167 us -> 153 us (0.916)
  the two profiles are of different devices: /device:TPU:120 before, /device:TPU:1 now
where the time goes in v4:
time: 153 us; the launch traced here: 150 us
  Pallas kernels  146 us (95%)
  local copies, waits for them, and re-layouts  3.55 us (2%)
    pallas_call x1, Pallas kernels, body(): pl.pallas_call(step_kernel, out_shape=(jax.ShapeDtypeStruct((BLK // 4, wi...  146 us
    unnamed x2, local copies, waits for them, and re-layouts  3.55 us

profile of v4, /device:TPU:1, one launch (start us, length us, event | category | flops | bytes accessed | tf_op | source)
XLA Modules:
  0.0 149.8 jit_solution(7595309855335434084)
XLA Ops:
  0.6 145.6 %step.1 = (bf16[64,2048]{1,0:T(8,128)(2,1)}, bf16[128,2048]{1,0:T(8,128)(2,1)}) custom-call(bf16[256,512]{1,0:T(8,128)(2,1)} %query_ref.1, bf16[256,128]{1,0:T(8,128)(2,1)} %key_ref.1, bf16[256,128]{1,0:T(8,128)(2,1)} %value_ref.1, bf16[2,256]{1,0:T(2,128)(2,1)} %bitcast.5, f32[8]{0:T(128)} %offset_ref.1, bf16[128,2048]{1,0:T(8,128)(2,1)} %x_ref.1, ...), custom_call_target="tpu_custom_call" | custom-call | tf_op jit(solution)/shard_map/step/pallas_call | solution.py:638
  146.3 1.7 %copy.17 = bf16[64,2048]{1,0:T(8,128)(2,1)} copy(bf16[64,2048]{1,0:T(8,128)(2,1)} %get-tuple-element.4) | data formatting | bytes 524288
  147.9 1.9 %copy.18 = bf16[128,2048]{1,0:T(8,128)(2,1)} copy(bf16[128,2048]{1,0:T(8,128)(2,1)} %get-tuple-element.5) | data formatting | bytes 1048576

commit v5 on v4

--- a/solution.py
+++ b/solution.py
@@ -103,6 +103,9 @@
     far_in,
     pair_send,
     pair_recv,
+    near_out,
+    nb_send,
+    nb_recv,
 ):
     me = lax.axis_index("ep")
     x = lax.axis_index("tp")
@@ -268,10 +271,7 @@
         remote(query_ref, guest, pair_send.at[0], pair_recv.at[0], partner)
 
     def gather_start(k):
-        if k == 0:
-            arrived(rx.at[0, pl.ds(0, 21)], a2a_recv.at[0])
-        else:
-            arrived(rx.at[k, pl.ds(0, 24)], a2a_recv.at[k])
+        arrived(rx.at[k, pl.ds(0, 21 if k == 0 else 24)], a2a_recv.at[k])
         own = rx.at[k, pl.ds(0, 24)]
         remote(own, rx.at[k, pl.ds(24, 24)], ag_send.at[k, 0], ag_recv.at[k, 0], {"tp": right})
         remote(own, rx.at[k, pl.ds(48, 24)], ag_send.at[k, 1], ag_recv.at[k, 1], {"tp": left})
@@ -327,29 +327,45 @@
             return 0
 
         lax.fori_loop(0, 8, down, 0)
+        if k == 0:
+
+            def send_near(i, _):
+                j = lax.rem(place + i, 8)
+                for c in range(4):
+                    remote(
+                        ys.at[0, pl.ds(24 * c + j * 3, 3)],
+                        near_out.at[c, pl.ds(place * 3, 3)],
+                        nb_send,
+                        nb_recv,
+                        {"ep": plane * 8 + j},
+                    )
+                return 0
+
+            lax.fori_loop(1, 8, send_near, 0)
+            for c in range(4):
+                near_out[c, pl.ds(place * 3, 3)] = ys[0, pl.ds(24 * c + place * 3, 3)]
+        else:
+            reduce_start(k)
+
+    def part(k, slot, at, count):
+        if k == 0:
+            return near_out.at[slot, pl.ds(at, count)]
+        return ys.at[k, pl.ds(24 * slot + at, count)]
+
+    def reduce_start(k):
+        if k == 0:
+            arrived(rx.at[0, pl.ds(0, 84)], nb_recv)
+        remote(part(k, 3, 0, 12), first.at[k, 0], r1_send.at[k, 0], r1_recv.at[k, 0], {"tp": right})
+        remote(part(k, 3, 12, 12), first.at[k, 1], r1_send.at[k, 1], r1_recv.at[k, 1], {"tp": left})
         remote(
-            ys.at[k, pl.ds(72, 12)],
-            first.at[k, 0],
-            r1_send.at[k, 0],
-            r1_recv.at[k, 0],
-            {"tp": right},
-        )
-        remote(
-            ys.at[k, pl.ds(84, 12)],
-            first.at[k, 1],
-            r1_send.at[k, 1],
-            r1_recv.at[k, 1],
-            {"tp": left},
-        )
-        remote(
-            ys.at[k, pl.ds(60, 12)],
+            part(k, 2, 12, 12),
             fin.at[k, 0, pl.ds(12, 12)],
             rd_send.at[k, 0],
             fin_recv.at[k, 0],
             {"tp": right},
         )
         remote(
-            ys.at[k, pl.ds(24, 12)],
+            part(k, 1, 0, 12),
             fin.at[k, 1, pl.ds(0, 12)],
             rd_send.at[k, 1],
             fin_recv.at[k, 1],
@@ -357,11 +373,11 @@
         )
 
     def added(k):
-        for side, at, device in ((0, 48, right), (1, 36, left)):
+        for side, slot, at, device in ((0, 2, 0, right), (1, 1, 12, left)):
             arrived(first.at[k, side], r1_recv.at[k, side])
 
-            def add(i, _, side=side, at=at):
-                both = ys[k, pl.ds(at + 2 * i, 2)].astype(jnp.float32) + first[
+            def add(i, _, side=side, slot=slot, at=at):
+                both = part(k, slot, at + 2 * i, 2)[...].astype(jnp.float32) + first[
                     k, side, pl.ds(2 * i, 2)
                 ].astype(jnp.float32)
                 mid[k, side, pl.ds(2 * i, 2)] = both.astype(jnp.bfloat16)
@@ -383,13 +399,18 @@
         arrived(fin.at[k, 1, pl.ds(12, 12)], fin_recv.at[k, 3])
 
         def add(i, _):
-            total = ys[k, pl.ds(2 * i, 2)].astype(jnp.float32)
+            total = part(k, 0, 2 * i, 2)[...].astype(jnp.float32)
             total = total + fin[k, 0, pl.ds(2 * i, 2)].astype(jnp.float32)
             total = total + fin[k, 1, pl.ds(2 * i, 2)].astype(jnp.float32)
-            res[k, pl.ds(2 * i, 2)] = total.astype(jnp.bfloat16)
+            if k == 0:
+                r4[pl.ds(plane * 24 + 2 * i, 2)] = total.astype(jnp.bfloat16)
+            else:
+                res[k, pl.ds(2 * i, 2)] = total.astype(jnp.bfloat16)
             return 0
 
         lax.fori_loop(0, 12, add, 0)
+        if k == 0:
+            return
         far = lax.rem(plane + 4 - OFFSETS[k], 4) * 8
 
         def send_back(i, _):
@@ -403,9 +424,7 @@
             )
             return 0
 
-        lax.fori_loop(1 if k == 0 else 0, 8, send_back, 0)
-        if k == 0:
-            r4[pl.ds(me * 3, 3)] = res[0, pl.ds(place * 3, 3)]
+        lax.fori_loop(0, 8, send_back, 0)
 
     def queries(source):
         lane = iota((1, 128), 1)
@@ -536,24 +555,27 @@
     keys_core()
     gather_forward(2)
     expert(1)
-    added(0)
     gather_forward(3)
+    keys_here()
+    attend_start()
+    attend(0,2)
     expert(2)
     added(1)
-    back(0)
     expert(3)
     added(2)
-    keys_here()
-    attend_start()
-    attend(0, 4)
+    attend(2,5)
     added(3)
-    attend(4, 8)
+    reduce_start(0)
+    attend(5,8)
     back(1)
-    attend(8, 13)
+    attend(8,10)
     back(2)
-    attend(13, 15)
+    attend(10,13)
+    added(0)
     back(3)
-    attend(15, 17)
+    attend(13,15)
+    back(0)
+    attend(15,17)
     project()
 
     arrived(o4.at[pl.ds(0, 93)], a2a_send)
@@ -572,10 +594,12 @@
     for d in range(4):
         arrived(kt_z(0), kc_send.at[d, 0])
         arrived(vv_z(0), kc_send.at[d, 1])
-    arrived(o4.at[pl.ds(0, 93)], ret_send)
-
-    for k in range(4):
-        arrived(r4.at[pl.ds(0, 21 if k == 0 else 24)], ret_recv.at[k])
+    arrived(o4.at[pl.ds(0, 72)], ret_send)
+    arrived(rx.at[0, pl.ds(0, 84)], nb_send)
+
+    for k in (1, 2, 3, 0):
+        if k > 0:
+            arrived(r4.at[pl.ds(0, 24)], ret_recv.at[k])
         far = lax.rem(plane + OFFSETS[k], 4) * 24
 
         def unpack_back(i, _, far=far):
@@ -697,6 +721,9 @@
             vmem((4 * BLK, 2 * HD), bf16),
             dma((2,)),
             dma((2,)),
+            vmem((4, 24, 4, width), bf16),
+            dma,
+            dma,
         ],
         compiler_params=pltpu.CompilerParams(
             vmem_limit_bytes=63 * 1024 * 1024, collective_id=0, has_side_effects=True

time: 153 us -> 148 us (0.967); the launches traced: 150 us -> 147 us
  Pallas kernels: 146 us -> 143 us
    pallas_call x1, Pallas kernels: 146 us -> 143 us  [body(): pl.pallas_call(step_kernel, out_shape=(jax.ShapeDtypeStruct((BLK // 4, wi...]
where the time goes in v5:
time: 148 us; the launch traced here: 147 us
  Pallas kernels  143 us (97%)
  local copies, waits for them, and re-layouts  3.55 us (2%)
    pallas_call x1, Pallas kernels, body(): pl.pallas_call(step_kernel, out_shape=(jax.ShapeDtypeStruct((BLK // 4, wi...  143 us
    unnamed x2, local copies, waits for them, and re-layouts  3.55 us

profile of v5, /device:TPU:1, one launch (start us, length us, event | category | flops | bytes accessed | tf_op | source)
XLA Modules:
  0.0 147.5 jit_solution(11680735865253326154)
XLA Ops:
  0.6 143.3 %step.1 = (bf16[64,2048]{1,0:T(8,128)(2,1)}, bf16[128,2048]{1,0:T(8,128)(2,1)}) custom-call(bf16[256,512]{1,0:T(8,128)(2,1)} %query_ref.1, bf16[256,128]{1,0:T(8,128)(2,1)} %key_ref.1, bf16[256,128]{1,0:T(8,128)(2,1)} %value_ref.1, bf16[2,256]{1,0:T(2,128)(2,1)} %bitcast.5, f32[8]{0:T(128)} %offset_ref.1, bf16[128,2048]{1,0:T(8,128)(2,1)} %x_ref.1, ...), custom_call_target="tpu_custom_call" | custom-call | tf_op jit(solution)/shard_map/step/pallas_call | solution.py:662
  143.9 1.7 %copy.17 = bf16[64,2048]{1,0:T(8,128)(2,1)} copy(bf16[64,2048]{1,0:T(8,128)(2,1)} %get-tuple-element.4) | data formatting | bytes 524288
  145.6 1.9 %copy.18 = bf16[128,2048]{1,0:T(8,128)(2,1)} copy(bf16[128,2048]{1,0:T(8,128)(2,1)} %get-tuple-element.5) | data formatting | bytes 1048576
